TPU v7x, 128 devices: a whole 4x4x4 slice. The times are simulated.
128 devices in a mesh: sp: 16 (over z, y), dp: 8 (over x, core).
Axes of the slice: x: 4, y: 4, z: 4, core: 2. Of those that a mesh axis runs over, the one named last changes fastest.
Arguments:
- stream: bfloat16 [8, 2048, 2048], P('dp', 'sp'), may hold values from -1.796875 to 1.796875
- query_rows: bfloat16 [8, 2048, 2048], P('dp', 'sp'), may hold values from -5 to 5
- key_rows: bfloat16 [8, 2048, 2048], P('dp', 'sp'), may hold values from -5 to 5
- value_rows: bfloat16 [8, 2048, 2048], P('dp', 'sp'), may hold values from -6 to 6
- forget_sums: float32 [8, 16, 2048], P('dp', 'sp'), may hold values from -2048 to 0, as said below
- out_weight: bfloat16 [2048, 2048], replicated, may hold values from -1.5 to 1.5
- first_gain: float32 [2048], replicated, may hold values from 0.1 to 1.9
- expert_ids: int32 [8, 2048, 4], P('dp', 'sp'), may hold values from 0 to 127, all different within a row; in each aligned block of 128 rows (0 to 127, 128 to 255, ..., all dimensions but the last counted through in order) at most 6 rows name the same one
- route_scores: float32 [8, 2048, 4], P('dp', 'sp'), may hold values from -6 to 6
- gate_weight: bfloat16 [128, 2048, 512], P(('sp', 'dp')), may hold values from -0.5 to 0.5
- up_weight: bfloat16 [128, 2048, 512], P(('sp', 'dp')), may hold values from -0.5 to 0.5
- down_weight: bfloat16 [128, 512, 2048], P(('sp', 'dp')), may hold values from -0.0625 to 0.0625
- second_gain: float32 [2048], replicated, may hold values from 0.1 to 1.9
Outputs:
- mixed_stream: bfloat16 [8, 2048, 2048], P('dp', 'sp')
Inputs may be any that keep to these rules, and one draw needn't show every extreme that they name: `expert_ids`: each row names 4 different experts; in the rows of one device no expert is named more than 6 times. `forget_sums`: along positions each head's values never rise.
All inputs are finite; a program needn't handle non-finite values.
Results may differ from a plain program's by a relative error of at most 0.0085.
Values may be sent and summed in bfloat16 or wider, within the bound.
No kernel may reach another device: no remote copies, remote signals or barrier semaphores. Data moves between devices by JAX's collectives and lax.ppermute only.
A program may use at most 128 MiB of HBM per device.

v0:
```python
import jax
import jax.numpy as jnp
from jax import lax
from jax.sharding import Mesh
from jax.sharding import PartitionSpec as P

SP = ("sp_0", "sp_1")
SP_DP = ("sp_0", "sp_1", "dp")


deep_alpha = 8.0**0.25
clamp_limit = 7.0
swish_alpha = 1.702
norm_eps = 1e-05
mask_fill = -1e30


def sent_together(arrays, axis, split_dim, concat_dim, along):
    widths = [a.shape[along] for a in arrays]
    both = jnp.concatenate(arrays, axis=along)
    out = lax.all_to_all(both, axis, split_axis=split_dim, concat_axis=concat_dim, tiled=True)
    return tuple(jnp.split(out, [sum(widths[:k]) for k in range(1, len(widths))], axis=along))


def in_blocks(x, dim, count):
    before, after = (x.shape[:dim], x.shape[dim + 1 :])
    return jnp.moveaxis(x.reshape(*before, count, -1, *after), dim, 0)


def laid_out(tiles, dim):
    shape = list(tiles.shape[1:])
    shape[dim] *= tiles.shape[0]
    return jnp.moveaxis(tiles, 0, dim).reshape(shape)


def turned_blocks(tiles, axes, turns):
    inside = tiles.shape[1:]
    out = tiles.reshape(*(lax.axis_size(a) for a in axes), *inside)
    for k in turns:
        out = lax.all_to_all(out, axes[k], k, k, tiled=True)
    return out.reshape(-1, *inside)


def stepwise_exchange(x, axes, turns, split_dim, concat_dim):
    tiles = in_blocks(x, split_dim, lax.axis_size(axes))
    return laid_out(turned_blocks(tiles, axes, turns), concat_dim)


def layer_norm(summed, gain_row):
    centre = jnp.mean(summed, axis=-1, keepdims=True)
    spread = jnp.mean(jnp.square(summed - centre), axis=-1, keepdims=True)
    return (summed - centre) * lax.rsqrt(spread + norm_eps) * gain_row


def attend_local(query_all, key_all, value_all, gate_all):
    length, width = query_all.shape
    heads = gate_all.shape[0]
    head_size = width // heads
    query_split = query_all.reshape(length, heads, head_size)
    key_split = key_all.reshape(length, heads, head_size)
    value_split = value_all.reshape(length, heads, head_size)
    q_block = min(512, length)
    block_count = length // q_block
    inv_root = head_size ** (-0.5)
    key_pos = jnp.arange(length, dtype=jnp.int32)

    def one_block(block_index):
        first_row = block_index * q_block
        row_block = lax.dynamic_slice_in_dim(query_split, first_row, q_block, 0)
        row_gate = lax.dynamic_slice_in_dim(gate_all, first_row, q_block, 1)
        scores = (
            jnp.einsum("qhd,khd->hqk", row_block, key_split, preferred_element_type=jnp.float32)
            * inv_root
        )
        scores = scores + row_gate[:, :, None] - gate_all[:, None, :]
        query_pos = first_row + jnp.arange(q_block, dtype=jnp.int32)
        scores = jnp.where((query_pos[:, None] >= key_pos[None, :])[None], scores, mask_fill)
        row_max = jnp.max(scores, axis=2, keepdims=True)
        weights = jnp.exp(scores - row_max)
        row_total = jnp.sum(weights, axis=2)
        blended = jnp.einsum(
            "hqk,khd->qhd",
            weights.astype(jnp.bfloat16),
            value_split,
            preferred_element_type=jnp.float32,
        )
        return (blended / row_total.T[:, :, None]).astype(jnp.bfloat16)

    return lax.map(one_block, jnp.arange(block_count, dtype=jnp.int32)).reshape(length, width)


def expert_rows(row_block, gate_matrix, up_matrix, down_matrix):
    gate_act = jnp.minimum(
        jnp.dot(row_block, gate_matrix, preferred_element_type=jnp.float32), clamp_limit
    )
    up_act = jnp.clip(
        jnp.dot(row_block, up_matrix, preferred_element_type=jnp.float32), -clamp_limit, clamp_limit
    )
    hidden = (gate_act * jax.nn.sigmoid(swish_alpha * gate_act) * (up_act + 1.0)).astype(
        jnp.bfloat16
    )
    return jnp.dot(hidden, down_matrix, preferred_element_type=jnp.float32).astype(jnp.bfloat16)


def shards(
    stream,
    query_rows,
    key_rows,
    value_rows,
    forget_sums,
    out_weight,
    first_gain,
    expert_ids,
    route_scores,
    gate_weight,
    up_weight,
    down_weight,
    second_gain,
):
    q_heads, k_heads, v_heads = sent_together((query_rows, key_rows, value_rows), SP, 2, 1, 0)
    attended = attend_local(q_heads[0], k_heads[0], v_heads[0], forget_sums[0])[None]
    returned_rows = stepwise_exchange(attended, SP, (0, 1), 1, 2)
    projected = jnp.dot(returned_rows[0], out_weight, preferred_element_type=jnp.float32)
    first_stream = layer_norm(
        deep_alpha * stream[0].astype(jnp.float32) + projected, first_gain
    ).astype(jnp.bfloat16)
    tokens_here = expert_ids.shape[1]
    top_k = expert_ids.shape[2]
    model_width = first_stream.shape[1]
    sp_count = lax.axis_size(SP)
    dp_count = lax.axis_size("dp")
    expert_count = sp_count * dp_count
    capacity = max(2, 3 * tokens_here * top_k // (2 * expert_count))
    flat_ids = expert_ids[0].reshape(-1)
    one_hot = (flat_ids[:, None] == jnp.arange(expert_count, dtype=jnp.int32)[None, :]).astype(
        jnp.int32
    )
    slot_ids = jnp.sum((jnp.cumsum(one_hot, axis=0) - one_hot) * one_hot, axis=1)
    slot_index = flat_ids * capacity + slot_ids
    slot_range = jnp.arange(expert_count * capacity, dtype=jnp.int32)
    matches = slot_range[:, None] == slot_index[None, :]
    dispatch = jnp.sum(matches.astype(jnp.int32).reshape(-1, tokens_here, top_k), axis=2).astype(
        jnp.bfloat16
    )
    outgoing = jnp.dot(dispatch, first_stream, preferred_element_type=jnp.float32).astype(
        jnp.bfloat16
    )
    outgoing = outgoing.reshape(expert_count, capacity, model_width)
    arrived = lax.all_to_all(outgoing, SP_DP, split_axis=0, concat_axis=0, tiled=True)
    finished = expert_rows(
        arrived.reshape(-1, model_width), gate_weight[0], up_weight[0], down_weight[0]
    )
    returned = lax.all_to_all(
        finished.reshape(arrived.shape), SP_DP, split_axis=0, concat_axis=0, tiled=True
    )
    route_weights = jax.nn.softmax(route_scores[0], axis=-1).reshape(-1)
    combine = jnp.sum(
        jnp.where(matches, route_weights[None, :], 0.0).reshape(-1, tokens_here, top_k), axis=2
    )
    mixture = lax.dot_general(
        combine,
        returned.reshape(-1, model_width).astype(jnp.float32),
        (((0,), (0,)), ((), ())),
        preferred_element_type=jnp.float32,
    )
    second = layer_norm(deep_alpha * first_stream.astype(jnp.float32) + mixture, second_gain)
    return second.astype(jnp.bfloat16)[None]


def solution(mesh):
    finer = Mesh(mesh.devices.reshape(4, 4, mesh.shape["dp"]), ("sp_0", "sp_1", "dp"))
    placed = (
        P("dp", SP, None),
        P("dp", SP, None),
        P("dp", SP, None),
        P("dp", SP, None),
        P("dp", SP, None),
        P(),
        P(),
        P("dp", SP, None),
        P("dp", SP, None),
        P(SP_DP, None, None),
        P(SP_DP, None, None),
        P(SP_DP, None, None),
        P(),
    )
    return jax.shard_map(
        shards, mesh=finer, in_specs=placed, out_specs=P("dp", SP, None), check_vma=False
    )
```

profile of v0, /device:TPU:1, one launch (start us, length us, event | category | flops | bytes accessed | tf_op | source)
XLA Modules:
  0.0 280.6 jit_solution(16629972950143782536)
XLA Ops:
  0.0 2.5 copy.68
  2.5 3.6 %copy.69 = bf16[1,128,2048]{1,0,2:T(2,128)(2,1)} copy(bf16[1,128,2048]{2,1,0:T(8,128)(2,1)} %param.17) | data formatting | bytes 1048576 | tf_op args[2]
  6.1 3.6 %copy.70 = bf16[1,128,2048]{1,0,2:T(2,128)(2,1)} copy(bf16[1,128,2048]{2,1,0:T(8,128)(2,1)} %param.18) | data formatting | bytes 1048576 | tf_op args[3]
  9.7 5.9 %pad_maximum_fusion = bf16[3,128,2048]{1,0,2:T(4,128)(2,1)} fusion(bf16[1,128,2048]{1,0,2:T(2,128)(2,1)} %copy.70, bf16[1,128,2048]{1,0,2:T(2,128)(2,1)} %copy.69, bf16[1,128,2048]{1,0,2:T(2,128)(2,1)S(1)} %copy.68), kind=kLoop, calls=%fused_computation.24 | loop fusion | flops 4718592 | bytes 3145728 | tf_op jit(solution)/shard_map/concatenate | solution.py:20
  15.6 8.8 %all-to-all-start = ((bf16[3,128,2048]{1,0,2:T(4,128)(2,1)}), bf16[3,128,2048]{1,0,2:T(4,128)(2,1)}, u32[]{:S(2)}, u32[]{:S(2)}) async-start(bf16[3,128,2048]{1,0,2:T(4,128)(2,1)} %pad_maximum_fusion), calls=%async_computation | async-start | bytes 4194304 | tf_op jit(solution)/shard_map/all_to_all | solution.py:21
  24.4 0.1 copy.78
  24.5 0.1 eq.45
  24.6 0.1 eq.41
  24.7 0.1 copy.81
  24.8 0.2 fusion.43
  25.0 30.3 %all-to-all-done = bf16[3,128,2048]{1,0,2:T(4,128)(2,1)} async-done(((bf16[3,128,2048]{1,0,2:T(4,128)(2,1)}), bf16[3,128,2048]{1,0,2:T(4,128)(2,1)}, u32[]{:S(2)}, u32[]{:S(2)}) %all-to-all-start) | async-done | bytes 1572896 | tf_op jit(solution)/shard_map/all_to_all | solution.py:21
  55.4 1.8 copy.71
  57.2 0.0 copy-start.3
  57.2 0.9 fusion.55
  58.1 2.0 copy.72
  60.1 1.0 copy.73
  61.2 0.3 copy.74
  61.5 23.0 %while.11 = (s32[]{:T(128)}, bf16[4,512,1,128]{3,1,2,0:T(8,128)(2,1)}, s32[4]{0:T(128)S(1)}, bf16[2048,1,128]{2,0,1:T(8,128)(2,1)}, bf16[2048,1,128]{2,0,1:T(8,1...) while((s32[]{:T(128)}, ...), condition=%wide.region_3.4_spmd.clone, body=%wide.region_0.3_spmd.clone.sunk | while | flops 547487232 | bytes 13923003 | solution.py:89
  61.5 0.6 dynamic_slice.25
  62.7 2.4 fusion.71
  65.1 0.7 fusion.72
  65.8 1.5 fusion.73
  67.2 0.6 dynamic_slice.25
  68.4 2.4 fusion.71
  70.8 0.7 fusion.72
  71.5 1.5 fusion.73
  73.0 0.6 dynamic_slice.25
  74.2 2.4 fusion.71
  76.5 0.7 fusion.72
  77.3 1.5 fusion.73
  78.7 0.6 dynamic_slice.25
  79.9 2.4 fusion.71
  82.3 0.7 fusion.72
  83.0 1.5 fusion.73
  84.4 2.0 copy.75
  86.5 3.5 %all-to-all-start.1 = ((bf16[4,4,1,128,128]{3,4,1,2,0:T(8,128)(2,1)}), bf16[4,4,1,128,128]{3,4,1,2,0:T(8,128)(2,1)S(1)}, u32[]{:S(2)}, u32[]{:S(2)}) async-start(bf16[4,4,1,128,128]{3,4,1,2,0:T(8,128)(2,1)} %copy.75), calls=%async_computation.1 | async-start | bytes 1048576 | tf_op jit(solution)/shard_map/all_to_all | solution.py:40
  90.1 7.4 %all-to-all-done.1 = bf16[4,4,1,128,128]{3,4,1,2,0:T(8,128)(2,1)S(1)} async-done(((bf16[4,4,1,128,128]{3,4,1,2,0:T(8,128)(2,1)}), bf16[4,4,1,128,128]{3,4,1,2,0:T(8,128)(2,1)S(1)}, u32[]{:S(2)}, u32[]{:S(2)}) %all-to-all-start.1) | async-done | bytes 524320 | tf_op jit(solution)/shard_map/all_to_all | solution.py:40
  97.4 0.8 copy.76
  98.3 3.5 %all-to-all-start.2 = ((bf16[4,4,1,128,128]{3,4,0,2,1:T(8,128)(2,1)}), bf16[4,4,1,128,128]{3,4,0,2,1:T(8,128)(2,1)S(1)}, u32[]{:S(2)}, u32[]{:S(2)}) async-start(bf16[4,4,1,128,128]{3,4,0,2,1:T(8,128)(2,1)} %copy.76), calls=%async_computation.2 | async-start | bytes 1048576 | tf_op jit(solution)/shard_map/all_to_all | solution.py:40
  101.7 0.2 fusion.42
  102.0 0.1 reduce_sum.86
  102.1 0.1 copy.83
  102.2 0.2 convert_reduce_fusion
  102.4 6.3 %all-to-all-done.2 = bf16[4,4,1,128,128]{3,4,0,2,1:T(8,128)(2,1)S(1)} async-done(((bf16[4,4,1,128,128]{3,4,0,2,1:T(8,128)(2,1)}), bf16[4,4,1,128,128]{3,4,0,2,1:T(8,128)(2,1)S(1)}, u32[]{:S(2)}, u32[]{:S(2)}) %all-to-all-start.2) | async-done | bytes 524320 | tf_op jit(solution)/shard_map/all_to_all | solution.py:40
  108.7 0.0 copy-start.1
  108.7 4.8 %fusion.56 = (f32[128]{0:T(128)S(1)}, f32[128,2048]{1,0:T(8,128)S(1)}) fusion(bf16[128,2048]{0,1:T(8,128)(2,1)S(1)} %bitcast.111, bf16[2048,2048]{1,0:T(8,128)(2,1)} %param.20, bf16[1,128,2048]{2,1,0:T(8,128)(2,1)} %param.15), kind=kOutput, calls=%fused_computation.69 | convolution fusion | flops 1074790272 | bytes 10486272 | tf_op jit(solution)/shard_map/dot_general | solution.py:123
  113.5 0.3 multiply_reduce_fusion.1
  113.8 0.0 copy-start.5
  113.8 0.5 copy-done.5
  114.3 2.7 convolution_convert_fusion.1
  117.1 6.3 %reshape.164 = bf16[128,6,2048]{2,1,0:T(8,128)(2,1)} reshape(bf16[768,2048]{1,0:T(8,128)(2,1)} %convolution_convert_fusion.1) | data formatting | bytes 6291456 | tf_op jit(solution)/shard_map/reshape | solution.py:148
  123.3 62.2 %all_to_all.35 = bf16[128,6,2048]{2,1,0:T(8,128)(2,1)} all-to-all(bf16[128,6,2048]{2,1,0:T(8,128)(2,1)} %reshape.164), channel_id=1, replica_groups=mesh['sp_0'=4,'sp_1'=4,'dp'=8] {'sp_0','sp_1','dp'}, dimensions={0} | all-to-all | bytes 6291456 | tf_op jit(solution)/shard_map/all_to_all | solution.py:149
  185.5 6.3 %reshape.165 = bf16[768,2048]{1,0:T(8,128)(2,1)} reshape(bf16[128,6,2048]{2,1,0:T(8,128)(2,1)} %all_to_all.35) | data formatting | bytes 6291456 | tf_op jit(solution)/shard_map/reshape | solution.py:151
  191.8 5.5 %fusion.30 = f32[768,512]{1,0:T(8,128)} fusion(bf16[768,2048]{1,0:T(8,128)(2,1)} %reshape.165, bf16[1,2048,512]{2,1,0:T(8,128)(2,1)} %param.24), kind=kOutput, calls=%fused_computation.28 | convolution fusion | flops 1610612736 | bytes 6815744 | tf_op jit(solution)/shard_map/dot_general | solution.py:94
  197.3 8.4 %convolution_convert_fusion = bf16[768,2048]{1,0:T(8,128)(2,1)} fusion(bf16[1,512,2048]{2,1,0:T(8,128)(2,1)S(1)} %copy-done, f32[768,512]{1,0:T(8,128)} %fusion.30, bf16[768,2048]{1,0:T(8,128)(2,1)} %reshape.165, bf16[1,2048,512]{2,1,0:T(8,128)(2,1)} %param.25), kind=kOutput, calls=%fused_computation.20 | convolution fusion | flops 3226730496 | bytes 12058624 | tf_op jit(solution)/shard_map/dot_general | solution.py:102
  205.7 6.3 %reshape.166 = bf16[128,6,2048]{2,1,0:T(8,128)(2,1)} reshape(bf16[768,2048]{1,0:T(8,128)(2,1)} %convolution_convert_fusion) | data formatting | bytes 6291456 | tf_op jit(solution)/shard_map/reshape | solution.py:154
  212.0 5.6 %all-to-all-start.4 = ((bf16[128,6,2048]{2,1,0:T(8,128)(2,1)}), bf16[128,6,2048]{2,1,0:T(8,128)(2,1)}, u32[]{:S(2)}, u32[]{:S(2)}) async-start(bf16[128,6,2048]{2,1,0:T(8,128)(2,1)} %reshape.166), calls=%async_computation.4 | async-start | bytes 8388608 | tf_op jit(solution)/shard_map/all_to_all | solution.py:153
  217.7 0.2 select_reduce_fusion
  217.8 0.0 copy-start.6
  217.8 52.5 %all-to-all-done.4 = bf16[128,6,2048]{2,1,0:T(8,128)(2,1)} async-done(((bf16[128,6,2048]{2,1,0:T(8,128)(2,1)}), bf16[128,6,2048]{2,1,0:T(8,128)(2,1)}, u32[]{:S(2)}, u32[]{:S(2)}) %all-to-all-start.4) | async-done | bytes 3145760 | tf_op jit(solution)/shard_map/all_to_all | solution.py:153
  270.3 6.3 %reshape.167 = bf16[768,2048]{1,0:T(8,128)(2,1)} reshape(bf16[128,6,2048]{2,1,0:T(8,128)(2,1)} %all-to-all-done.4) | data formatting | bytes 6291456 | tf_op jit(solution)/shard_map/reshape | solution.py:162
  276.6 2.7 fusion.57
  279.3 0.3 multiply_reduce_fusion
  279.6 1.0 fusion.40
  (36 shorter events, 0.3 us)
Async XLA Ops:
  0.0 197.3 %copy-start = (bf16[1,512,2048]{2,1,0:T(8,128)(2,1)S(1)}, bf16[1,512,2048]{2,1,0:T(8,128)(2,1)}, u32[]{:S(2)}) copy-start(bf16[1,512,2048]{2,1,0:T(8,128)(2,1)} %param.26) | copy-start | bytes 6291460
  15.6 8.8 %copy-start.7 = (s32[1,128,4]{1,2,0:T(4,128)S(1)}, s32[1,128,4]{1,2,0:T(4,128)}, u32[]{:S(2)}) copy-start(s32[1,128,4]{1,2,0:T(4,128)} %param.22) | copy-start | bytes 6148
  15.6 39.8 %all-to-all-start = ((bf16[3,128,2048]{1,0,2:T(4,128)(2,1)}), bf16[3,128,2048]{1,0,2:T(4,128)(2,1)}, u32[]{:S(2)}, u32[]{:S(2)}) async-start(bf16[3,128,2048]{1,0,2:T(4,128)(2,1)} %pad_maximum_fusion), calls=%async_computation | async-start | bytes 4194304 | tf_op jit(solution)/shard_map/all_to_all | solution.py:21
  57.2 4.3 %copy-start.3 = (f32[1,1,2048]{2,1,0:T(1,128)S(1)}, f32[1,1,2048]{2,1,0:T(1,128)}, u32[]{:S(2)}) copy-start(f32[1,1,2048]{2,1,0:T(1,128)} %param.19) | copy-start | bytes 24580
  86.5 11.0 %all-to-all-start.1 = ((bf16[4,4,1,128,128]{3,4,1,2,0:T(8,128)(2,1)}), bf16[4,4,1,128,128]{3,4,1,2,0:T(8,128)(2,1)S(1)}, u32[]{:S(2)}, u32[]{:S(2)}) async-start(bf16[4,4,1,128,128]{3,4,1,2,0:T(8,128)(2,1)} %copy.75), calls=%async_computation.1 | async-start | bytes 1048576 | tf_op jit(solution)/shard_map/all_to_all | solution.py:40
  98.3 10.4 %all-to-all-start.2 = ((bf16[4,4,1,128,128]{3,4,0,2,1:T(8,128)(2,1)}), bf16[4,4,1,128,128]{3,4,0,2,1:T(8,128)(2,1)S(1)}, u32[]{:S(2)}, u32[]{:S(2)}) async-start(bf16[4,4,1,128,128]{3,4,0,2,1:T(8,128)(2,1)} %copy.76), calls=%async_computation.2 | async-start | bytes 1048576 | tf_op jit(solution)/shard_map/all_to_all | solution.py:40
  108.7 5.6 %copy-start.1 = (f32[2048]{0:T(1024)S(1)}, f32[2048]{0:T(1024)}, u32[]{:S(2)}) copy-start(f32[2048]{0:T(1024)} %param.21) | copy-start | bytes 24580
  113.8 0.5 copy-start.5
  212.0 5.6 %copy-start.2 = (f32[1,128,4]{1,2,0:T(4,128)S(1)}, f32[1,128,4]{1,2,0:T(4,128)}, u32[]{:S(2)}) copy-start(f32[1,128,4]{1,2,0:T(4,128)} %param.23) | copy-start | bytes 6148
  212.0 58.3 %all-to-all-start.4 = ((bf16[128,6,2048]{2,1,0:T(8,128)(2,1)}), bf16[128,6,2048]{2,1,0:T(8,128)(2,1)}, u32[]{:S(2)}, u32[]{:S(2)}) async-start(bf16[128,6,2048]{2,1,0:T(8,128)(2,1)} %reshape.166), calls=%async_computation.4 | async-start | bytes 8388608 | tf_op jit(solution)/shard_map/all_to_all | solution.py:153
  217.8 58.8 %copy-start.6 = (f32[128]{0:T(128)S(1)}, f32[128]{0:T(128)}, u32[]{:S(2)}) copy-start(f32[128]{0:T(128)} %copy-done.5) | copy-start | bytes 1540
  276.6 3.0 %copy-start.4 = (f32[2048]{0:T(1024)S(1)}, f32[2048]{0:T(1024)}, u32[]{:S(2)}) copy-start(f32[2048]{0:T(1024)} %param.27) | copy-start | bytes 24580
where the time goes:
time: 282 us; the launch traced here: 281 us
  waiting for transfers between devices  96.4 us (34%)
  blocking collectives  62.2 us (22%)
  local copies, waits for them, and re-layouts  47.4 us (17%)
  matrix products  39.5 us (14%)
  starting transfers between devices  21.3 us (8%)
  other arithmetic  11.2 us (4%)
    all_to_all x1, blocking collectives, shards(): lax.all_to_all(outgoing, SP_DP, split_axis=0, concat_axis=0, tiled=True)  62.2 us
    all_to_all x1, waiting for transfers between devices, shards(): lax.all_to_all(finished.reshape(arrived.shape), SP_DP, split_axis=0, conc...  52.5 us
    all_to_all x1, waiting for transfers between devices, sent_together(): lax.all_to_all(both, axis, split_axis=split_dim, concat_axis=concat_dim,...  30.3 us
    all_to_all x2, waiting for transfers between devices, turned_blocks(): out = lax.all_to_all(out, axes[k], k, k, tiled=True)  13.6 us
    unnamed x21, local copies, waits for them, and re-layouts  10.4 us
    dot_general x4, matrix products, one_block(): jnp.einsum('qhd,khd->hqk', row_block, key_split, preferred_element_type=j...  9.58 us
    all_to_all x1, starting transfers between devices, sent_together(): lax.all_to_all(both, axis, split_axis=split_dim, concat_axis=concat_dim,...  8.77 us
    dot_general x1, matrix products, expert_rows(): jnp.dot(hidden, down_matrix, preferred_element_type=jnp.float32)  8.38 us
  transfers between devices with their start and end apart: 4, of which 4 were waited for; matrix products, arithmetic and copies ran while one was open for 1% of the time, Pallas kernels for 0%

commit v1 on v0

v1 whole, which is shorter than its diff:
```python
import jax
import jax.numpy as jnp
from jax import lax
from jax.experimental import pallas as pl
from jax.experimental.pallas import tpu as pltpu
from jax.sharding import Mesh
from jax.sharding import PartitionSpec as P

SP = ("sp_0", "sp_1")
SP_DP = ("sp_0", "sp_1", "dp")

deep_alpha = 8.0**0.25
clamp_limit = 7.0
swish_alpha = 1.702
norm_eps = 1e-05
mask_fill = -1e30
log2_e = 1.4426950408889634

LANE = 128
SUB = 8
SLOTS = 6
MAIN = 12
TAIL = 4
MIB = 1 << 20


def call(body, out_shape, vmem_mib, **kwargs):
    return pl.pallas_call(
        body,
        out_shape=out_shape,
        compiler_params=pltpu.CompilerParams(vmem_limit_bytes=vmem_mib * MIB),
        **kwargs,
    )


def dot(a, b, dims=((1,), (0,))):
    return lax.dot_general(a, b, (dims, ((), ())), preferred_element_type=jnp.float32)


def layer_norm(summed, gain_row):
    centre = jnp.mean(summed, axis=-1, keepdims=True)
    centred = summed - centre
    spread = jnp.mean(jnp.square(centred), axis=-1, keepdims=True)
    return centred * lax.rsqrt(spread + norm_eps) * gain_row


def pack_heads_body(q_ref, k_ref, v_ref, out_ref):
    for h in range(out_ref.shape[0]):
        for n, ref in enumerate((q_ref, k_ref, v_ref)):
            out_ref[h, n] = ref[0, :, h * LANE : (h + 1) * LANE]


def pack_heads(q, k, v):
    rows, width = q.shape[1:]
    heads, step = width // LANE, 4
    spec = pl.BlockSpec((1, rows, step * LANE), lambda i: (0, 0, i))
    return call(
        pack_heads_body,
        jax.ShapeDtypeStruct((heads, 3, rows, LANE), q.dtype),
        16,
        grid=(heads // step,),
        in_specs=[spec] * 3,
        out_specs=pl.BlockSpec((step, 3, rows, LANE), lambda i: (i, 0, 0, 0)),
    )(q, k, v)


def attend_body(qkv_ref, gate_ref, out_ref, score_ref):
    parts, _, rows, size = qkv_ref.shape
    pair = 2
    block = pair * rows
    scale = size ** (-0.5) * log2_e
    for b in range(parts // pair):
        q = qkv_ref[pair * b : pair * (b + 1), 0].reshape(block, size)
        base = gate_ref[:, block * b : block * b + 1]
        top = jnp.full((block, LANE), mask_fill, jnp.float32)
        for j in range(b + 1):
            keys = qkv_ref[pair * j : pair * (j + 1), 1].reshape(block, size)
            bias = (gate_ref[:, block * j : block * (j + 1)] - base) * log2_e
            s = dot(q, keys, ((1,), (1,))) * scale - bias
            if j == b:
                row = lax.broadcasted_iota(jnp.int32, s.shape, 0)
                col = lax.broadcasted_iota(jnp.int32, s.shape, 1)
                s = jnp.where(row >= col, s, mask_fill)
            score_ref[:, block * j : block * (j + 1)] = s
            for c in range(block // LANE):
                top = jnp.maximum(top, s[:, c * LANE : (c + 1) * LANE])
        row_max = jnp.max(top, axis=1, keepdims=True)
        total = jnp.zeros((block, LANE), jnp.float32)
        blended = jnp.zeros((block, size), jnp.float32)
        for j in range(b + 1):
            w = jnp.exp2(score_ref[:, block * j : block * (j + 1)] - row_max)
            for c in range(block // LANE):
                total = total + w[:, c * LANE : (c + 1) * LANE]
            values = qkv_ref[pair * j : pair * (j + 1), 2].reshape(block, size)
            blended = blended + dot(w.astype(jnp.bfloat16), values)
        row_total = jnp.sum(total, axis=1, keepdims=True)
        done = (blended / row_total).astype(jnp.bfloat16)
        out_ref[pair * b : pair * (b + 1)] = done.reshape(pair, rows, size)


def attend(qkv, gates):
    parts, _, rows, size = qkv.shape
    return call(
        attend_body,
        jax.ShapeDtypeStruct((parts, rows, size), qkv.dtype),
        24,
        scratch_shapes=[pltpu.VMEM((2 * rows, parts * rows), jnp.float32)],
    )(qkv, gates)


def slot_of(place, kind):
    if kind == 0:
        return jnp.where(place < SLOTS, place, -2)
    return jnp.where(place >= SLOTS, place - SLOTS + 2 * (kind - 1), -2)


def route_body(ids_ref, score_ref, pick_ref, blend_ref):
    rows, top_k = ids_ref.shape[1:]
    experts = pick_ref.shape[1] // SUB
    expert = lax.broadcasted_iota(jnp.int32, (rows, experts), 1)
    scores = score_ref[0]
    raised = jnp.exp(scores - jnp.max(scores, axis=1, keepdims=True))
    shares = raised / jnp.sum(raised, axis=1, keepdims=True)
    named = jnp.zeros((rows, experts), jnp.float32)
    share = jnp.zeros((rows, experts), jnp.float32)
    for k in range(top_k):
        hit = ids_ref[0, :, k : k + 1] == expert
        named = jnp.where(hit, 1.0, named)
        share = jnp.where(hit, shares[:, k : k + 1], share)
    earlier = lax.broadcasted_iota(jnp.int32, (rows, rows), 0) > lax.broadcasted_iota(
        jnp.int32, (rows, rows), 1
    )
    rank = dot(jnp.where(earlier, 1.0, 0.0).astype(jnp.bfloat16), named.astype(jnp.bfloat16))
    slot = jnp.where(named > 0.0, rank, -1.0)
    by_expert = jnp.broadcast_to(slot.T[:, None, :], (experts, SUB, rows))
    place = lax.broadcasted_iota(jnp.int32, (experts, SUB, rows), 1)
    for kind in range(4):
        hit = by_expert == slot_of(place, kind).astype(jnp.float32)
        pick = jnp.where(hit, 1.0, 0.0).reshape(experts * SUB, rows).astype(jnp.bfloat16)
        pick_ref[kind] = pick
    wide = (experts, experts * SUB)
    spread = lax.broadcasted_iota(jnp.int32, wide, 0) == lax.broadcasted_iota(
        jnp.int32, wide, 1
    ) // SUB
    spread = jnp.where(spread, 1.0, 0.0).astype(jnp.bfloat16)
    wide_slot = dot(slot.astype(jnp.bfloat16), spread)
    wide_share = dot(share.astype(jnp.bfloat16), spread)
    place = lax.broadcasted_iota(jnp.int32, wide_slot.shape, 1) % SUB
    for kind in range(4):
        hit = wide_slot == slot_of(place, kind).astype(jnp.float32)
        blend_ref[kind] = jnp.where(hit, wide_share, 0.0).astype(jnp.bfloat16)


def route(ids, scores, experts):
    rows = ids.shape[1]
    return call(
        route_body,
        (
            jax.ShapeDtypeStruct((4, experts * SUB, rows), jnp.bfloat16),
            jax.ShapeDtypeStruct((4, rows, experts * SUB), jnp.bfloat16),
        ),
        24,
    )(ids, scores)


def project_body(heads_ref, stream_ref, weight_ref, gain_ref, pick_ref, first_ref, out_ref):
    heads = heads_ref.shape[0]
    experts = out_ref.shape[0]
    attended = jnp.concatenate([heads_ref[h] for h in range(heads)], axis=1)
    projected = dot(attended, weight_ref[...])
    summed = deep_alpha * stream_ref[0].astype(jnp.float32) + projected
    first = layer_norm(summed, gain_ref[...]).astype(jnp.bfloat16)
    first_ref[...] = first
    tail = first[:, MAIN * LANE :]
    for p in range(3):
        kept = [first[:, (3 * q + p) * LANE : (3 * q + p + 1) * LANE] for q in range(TAIL)]
        both = jnp.concatenate([jnp.concatenate(kept, axis=1), tail], axis=0)
        lhs = jnp.concatenate([pick_ref[0], pick_ref[p + 1]], axis=1)
        rows = dot(lhs, both).astype(jnp.bfloat16)
        for q in range(TAIL):
            tile = rows[:, q * LANE : (q + 1) * LANE]
            out_ref[:, 3 * q + p] = tile.reshape(experts, SUB, LANE)


def project(heads, stream, weight, gain, pick):
    rows, width = stream.shape[1:]
    experts = pick.shape[1] // SUB
    return call(
        project_body,
        (
            jax.ShapeDtypeStruct((rows, width), jnp.bfloat16),
            jax.ShapeDtypeStruct((experts, MAIN, SUB, LANE), jnp.bfloat16),
        ),
        36,
    )(heads, stream, weight, gain, pick)


def move_matrix(rows, p):
    to = lax.broadcasted_iota(jnp.int32, (rows, rows), 0)
    fro = lax.broadcasted_iota(jnp.int32, (rows, rows), 1)
    same = to // SUB == fro // SUB
    hit = same & (fro % SUB - SLOTS + 2 * p == to % SUB) & (fro % SUB >= SLOTS)
    return jnp.where(hit, 1.0, 0.0).astype(jnp.bfloat16)


def expert_body(in_ref, gate_ref, up_ref, down_ref, out_ref):
    sources = in_ref.shape[0]
    rows = sources * SUB
    kept = [in_ref[:, t].reshape(rows, LANE) for t in range(MAIN)]
    tail = jnp.zeros((rows, TAIL * LANE), jnp.float32)
    for p in range(3):
        spare = jnp.concatenate([kept[3 * q + p] for q in range(TAIL)], axis=1)
        tail = tail + dot(move_matrix(rows, p), spare)
    x = jnp.concatenate(kept + [tail.astype(jnp.bfloat16)], axis=1)
    gate_act = jnp.minimum(dot(x, gate_ref[0]), clamp_limit)
    up_act = jnp.clip(dot(x, up_ref[0]), -clamp_limit, clamp_limit)
    hidden = gate_act * jax.nn.sigmoid(swish_alpha * gate_act) * (up_act + 1.0)
    y = dot(hidden.astype(jnp.bfloat16), down_ref[0])
    y_tail = y[:, MAIN * LANE :].astype(jnp.bfloat16)
    own = lax.broadcasted_iota(jnp.int32, (rows, LANE), 0) % SUB < SLOTS
    for p in range(3):
        spare = dot(move_matrix(rows, p), y_tail, ((0,), (0,)))
        for q in range(TAIL):
            t = 3 * q + p
            tile = jnp.where(
                own, y[:, t * LANE : (t + 1) * LANE], spare[:, q * LANE : (q + 1) * LANE]
            )
            out_ref[:, t] = tile.astype(jnp.bfloat16).reshape(sources, SUB, LANE)


def expert(arrived, gate, up, down):
    sources, step = arrived.shape[0], 32
    block = pl.BlockSpec((step, MAIN, SUB, LANE), lambda i: (i, 0, 0, 0))
    whole = [pl.BlockSpec(w.shape, lambda i: (0, 0, 0)) for w in (gate, up, down)]
    return call(
        expert_body,
        jax.ShapeDtypeStruct(arrived.shape, arrived.dtype),
        36,
        grid=(sources // step,),
        in_specs=[block] + whole,
        out_specs=block,
    )(arrived, gate, up, down)


def combine_body(in_ref, blend_ref, first_ref, gain_ref, out_ref):
    experts = in_ref.shape[0]
    tail = None
    blocks = [None] * MAIN
    for p in range(3):
        rows = [in_ref[:, 3 * q + p].reshape(experts * SUB, LANE) for q in range(TAIL)]
        both = jnp.concatenate([blend_ref[0], blend_ref[p + 1]], axis=0)
        mixed = dot(both, jnp.concatenate(rows, axis=1))
        count = blend_ref.shape[1]
        for q in range(TAIL):
            blocks[3 * q + p] = mixed[:count, q * LANE : (q + 1) * LANE]
        tail = mixed[count:] if tail is None else tail + mixed[count:]
    mixture = jnp.concatenate(blocks + [tail], axis=1)
    summed = deep_alpha * first_ref[...].astype(jnp.float32) + mixture
    out_ref[0] = layer_norm(summed, gain_ref[...]).astype(jnp.bfloat16)


def combine(returned, blend, first, gain):
    return call(
        combine_body,
        jax.ShapeDtypeStruct((1, *first.shape), jnp.bfloat16),
        36,
    )(returned, blend, first, gain)


def exchange(x, axes):
    return lax.all_to_all(x, axes, split_axis=0, concat_axis=0, tiled=True)


def shards(
    stream,
    query_rows,
    key_rows,
    value_rows,
    forget_sums,
    out_weight,
    first_gain,
    expert_ids,
    route_scores,
    gate_weight,
    up_weight,
    down_weight,
    second_gain,
):
    experts = lax.axis_size(SP_DP)
    qkv = exchange(pack_heads(query_rows, key_rows, value_rows), SP)
    pick, blend = route(expert_ids, route_scores, experts)
    heads = exchange(attend(qkv, forget_sums[0]), SP)
    first, outgoing = project(heads, stream, out_weight, first_gain[None], pick)
    arrived = exchange(outgoing, SP_DP)
    finished = expert(arrived, gate_weight, up_weight, down_weight)
    returned = exchange(finished, SP_DP)
    return combine(returned, blend, first, second_gain[None])


def solution(mesh):
    finer = Mesh(mesh.devices.reshape(4, 4, mesh.shape["dp"]), ("sp_0", "sp_1", "dp"))
    rows = P("dp", SP, None)
    own = P(SP_DP, None, None)
    placed = (rows,) * 5 + (P(), P(), rows, rows, own, own, own, P())
    return jax.shard_map(shards, mesh=finer, in_specs=placed, out_specs=rows, check_vma=False)
```

time: 282 us -> 166 us (0.59)
  waiting for transfers between devices: 96.4 us -> 8.45 us
  blocking collectives: 62.2 us -> 125 us
  local copies, waits for them, and re-layouts: 47.4 us -> 6.79 us
  matrix products: 39.5 us -> 0 us
  Pallas kernels: 0 us -> 21.2 us
  starting transfers between devices: 21.3 us -> 3.57 us
  other arithmetic: 11.2 us -> 0 us
    all_to_all x4 -> x1, waiting for transfers between devices: 96.4 us -> 8.45 us  [exchange(): return lax.all_to_all(x, axes, split_axis=0, concat_axis=0, tiled=True)]
    all_to_all x1 -> x3, blocking collectives: 62.2 us -> 125 us  [exchange(): return lax.all_to_all(x, axes, split_axis=0, concat_axis=0, tiled=True)]
    dot_general x13 -> x0, matrix products: 39.5 us -> none  [the longest x4 9.58 us: one_block(): jnp.einsum('qhd,khd->hqk', row_block, key_split, preferred_element_type=j...]
    reshape x4 -> x0, local copies, waits for them, and re-layouts: 25.2 us -> none  [the longest x1 6.34 us: shards(): arrived.reshape(-1, model_width)]
    pallas_call x0 -> x6, Pallas kernels: none -> 21.2 us  [the longest x1 9.83 us: expert(): call(expert_body, jax.ShapeDtypeStruct(arrived.shape, arrived.dtype), 36,...]
    all_to_all x4 -> x1, starting transfers between devices: 21.3 us -> 3.57 us  [exchange(): return lax.all_to_all(x, axes, split_axis=0, concat_axis=0, tiled=True)]
    concatenate x1 -> x0, other arithmetic: 5.85 us -> none  [sent_together(): both = jnp.concatenate(arrays, axis=along)]
    split x4 -> x0, local copies, waits for them, and re-layouts: 4.25 us -> none  [sent_together(): jnp.split(out, [sum(widths[:k]) for k in range(1, len(widths))], axis=along)]
  transfers between devices with their start and end apart: 4 -> 1, of which waited for: 4 -> 1; matrix products, arithmetic and copies ran while one was open for 1% -> 0% of each run, Pallas kernels for 0% -> 1%
where the time goes in v1:
time: 166 us; the launch traced here: 165 us
  blocking collectives  125 us (75%)
  Pallas kernels  21.2 us (13%)
  waiting for transfers between devices  8.45 us (5%)
  local copies, waits for them, and re-layouts  6.79 us (4%)
  starting transfers between devices  3.57 us (2%)
    all_to_all x3, blocking collectives, exchange(): return lax.all_to_all(x, axes, split_axis=0, concat_axis=0, tiled=True)  125 us
    pallas_call x1, Pallas kernels, expert(): call(expert_body, jax.ShapeDtypeStruct(arrived.shape, arrived.dtype), 36,...  9.83 us
    all_to_all x1, waiting for transfers between devices, exchange(): return lax.all_to_all(x, axes, split_axis=0, concat_axis=0, tiled=True)  8.45 us
    unnamed x28, local copies, waits for them, and re-layouts  6.79 us
    pallas_call x1, Pallas kernels, attend(): call(attend_body, jax.ShapeDtypeStruct((parts, rows, size), qkv.dtype), 2...  5.38 us
    all_to_all x1, starting transfers between devices, exchange(): return lax.all_to_all(x, axes, split_axis=0, concat_axis=0, tiled=True)  3.57 us
  transfers between devices with their start and end apart: 1, of which 1 were waited for; matrix products, arithmetic and copies ran while one was open for 0% of the time, Pallas kernels for 1%

profile of v1, /device:TPU:1, one launch (start us, length us, event | category | flops | bytes accessed | tf_op | source)
XLA Modules:
  0.0 165.1 jit_solution(11440188577966266182)
XLA Ops:
  0.0 0.0 copy-start.5
  0.0 1.0 copy-done.5
  1.0 0.0 copy-start.6
  1.0 1.0 copy-done.6
  2.1 0.0 copy-start.7
  2.1 1.0 copy-done.7
  3.1 0.0 copy-start.8
  3.1 0.5 shard_map.127
  3.6 0.0 copy-start.11
  3.6 0.0 copy-start.12
  3.6 0.0 copy-start.4
  3.6 0.0 copy-start.10
  3.7 30.2 %all_to_all.20.qkv_ref = bf16[16,3,128,128]{3,2,1,0:T(8,128)(2,1)S(1)} all-to-all(bf16[16,3,128,128]{3,2,1,0:T(8,128)(2,1)S(1)} %shard_map.127), channel_id=1, replica_groups=mesh['sp_0'=4,'sp_1'=4,'dp'=8] {'sp_0','sp_1'}, dimensions={0} | all-to-all | bytes 3145728 | tf_op jit(solution)/shard_map/all_to_all | solution.py:271
  33.8 0.0 copy-done.8
  33.8 5.4 %shard_map.128 = bf16[16,128,128]{2,1,0:T(8,128)(2,1)} custom-call(bf16[16,3,128,128]{3,2,1,0:T(8,128)(2,1)S(1)} %all_to_all.20.qkv_ref, f32[1,2048]{1,0:T(1,128)S(1)} %bitcast.3), custom_call_target="tpu_custom_call" | custom-call | tf_op jit(solution)/shard_map/pallas_call | solution.py:103
  39.2 3.6 %all-to-all-start.1 = ((bf16[16,128,128]{2,1,0:T(8,128)(2,1)}), bf16[16,128,128]{2,1,0:T(8,128)(2,1)S(1)}, u32[]{:S(2)}, u32[]{:S(2)}) async-start(bf16[16,128,128]{2,1,0:T(8,128)(2,1)} %shard_map.128), calls=%async_computation.1 | async-start | bytes 1048576 | tf_op jit(solution)/shard_map/all_to_all | solution.py:271
  42.8 0.0 copy-done.11
  42.8 0.1 copy.14.ids_ref
  42.9 0.0 copy-done.12
  42.9 0.1 copy.15.score_ref
  43.0 0.9 shard_map.129
  43.9 8.5 %all-to-all-done.1.heads_ref = bf16[16,128,128]{2,1,0:T(8,128)(2,1)S(1)} async-done(((bf16[16,128,128]{2,1,0:T(8,128)(2,1)}), bf16[16,128,128]{2,1,0:T(8,128)(2,1)S(1)}, u32[]{:S(2)}, u32[]{:S(2)}) %all-to-all-start.1) | async-done | bytes 524320 | tf_op jit(solution)/shard_map/all_to_all | solution.py:271
  52.4 0.0 copy-done.4
  52.4 0.0 copy-done.10
  52.4 0.0 copy-start
  52.4 3.4 %copy-done = bf16[2048,2048]{1,0:T(8,128)(2,1)S(1)} copy-done((bf16[2048,2048]{1,0:T(8,128)(2,1)S(1)}, bf16[2048,2048]{1,0:T(8,128)(2,1)}, u32[]{:S(2)}) %copy-start) | copy-done | bytes 8388632
  55.8 2.5 %shard_map.130 = (bf16[128,2048]{1,0:T(8,128)(2,1)S(1)}, bf16[128,12,8,128]{3,2,1,0:T(8,128)(2,1)S(1)}) custom-call(bf16[16,128,128]{2,1,0:T(8,128)(2,1)S(1)} %all-to-all-done.1.heads_ref, bf16[1,128,2048]{2,1,0:T(8,128)(2,1)S(1)} %copy-done.4, bf16[2048,2048]{1,0:T(8,128)(2,1)S(1)} %copy-done, f32[1,2048]{1,0:T(1,128)S(1)} %bitcast.5, ...), custom_call_target="tpu_custom_call" | custom-call | tf_op jit(solution)/shard_map/pallas_call | solution.py:188
  58.3 0.0 copy-start.1
  58.3 0.0 copy-start.2
  58.3 0.0 copy-start.3
  58.3 49.2 %all_to_all.21.in_ref = bf16[128,12,8,128]{3,2,1,0:T(8,128)(2,1)S(1)} all-to-all(bf16[128,12,8,128]{3,2,1,0:T(8,128)(2,1)S(1)} %get-tuple-element.10), channel_id=1, replica_groups=mesh['sp_0'=4,'sp_1'=4,'dp'=8] {'sp_0','sp_1','dp'}, dimensions={0} | all-to-all | bytes 6291456 | tf_op jit(solution)/shard_map/all_to_all | solution.py:271
  107.6 0.0 copy-done.1
  107.6 0.0 copy-done.2
  107.6 0.0 copy-done.3
  107.6 9.8 %shard_map.131 = bf16[128,12,8,128]{3,2,1,0:T(8,128)(2,1)S(1)} custom-call(bf16[128,12,8,128]{3,2,1,0:T(8,128)(2,1)S(1)} %all_to_all.21.in_ref, bf16[1,2048,512]{2,1,0:T(8,128)(2,1)S(1)} %copy-done.1, bf16[1,2048,512]{2,1,0:T(8,128)(2,1)S(1)} %copy-done.2, bf16[1,512,2048]{2,1,0:T(8,128)(2,1)S(1)} %copy-done.3), custom_call_target="tpu_custom_call" | custom-call | tf_op jit(solution)/shard_map/pallas_call | solution.py:235
  117.4 0.0 copy-start.9
  117.4 45.6 %all_to_all.22.in_ref = bf16[128,12,8,128]{3,2,1,0:T(8,128)(2,1)S(1)} all-to-all(bf16[128,12,8,128]{3,2,1,0:T(8,128)(2,1)S(1)} %shard_map.131), channel_id=1, replica_groups=mesh['sp_0'=4,'sp_1'=4,'dp'=8] {'sp_0','sp_1','dp'}, dimensions={0} | all-to-all | bytes 6291456 | tf_op jit(solution)/shard_map/all_to_all | solution.py:271
  163.0 0.0 copy-done.9
  163.0 2.1 %shard_map.132 = bf16[1,128,2048]{2,1,0:T(8,128)(2,1)} custom-call(bf16[128,12,8,128]{3,2,1,0:T(8,128)(2,1)S(1)} %all_to_all.22.in_ref, bf16[4,128,1024]{2,1,0:T(8,128)(2,1)S(1)} %get-tuple-element.11.blend_ref, bf16[128,2048]{1,0:T(8,128)(2,1)S(1)} %get-tuple-element.12.first_ref, f32[1,2048]{1,0:T(1,128)S(1)} %bitcast.4), custom_call_target="tpu_custom_call" | custom-call | tf_op jit(solution)/shard_map/pallas_call | solution.py:263
Async XLA Ops:
  0.0 1.0 copy-start.5
  1.0 1.0 copy-start.6
  2.1 1.0 copy-start.7
  3.1 30.7 %copy-start.8 = (f32[1,1,2048]{2,1,0:T(1,128)S(1)}, f32[1,1,2048]{2,1,0:T(1,128)}, u32[]{:S(2)}) copy-start(f32[1,1,2048]{2,1,0:T(1,128)} %param.17) | copy-start | bytes 24580
  3.6 39.2 %copy-start.11 = (s32[1,128,4]{1,2,0:T(4,128)S(1)}, s32[1,128,4]{1,2,0:T(4,128)}, u32[]{:S(2)}) copy-start(s32[1,128,4]{1,2,0:T(4,128)} %param.20) | copy-start | bytes 6148
  3.6 39.3 %copy-start.12 = (f32[1,128,4]{1,2,0:T(4,128)S(1)}, f32[1,128,4]{1,2,0:T(4,128)}, u32[]{:S(2)}) copy-start(f32[1,128,4]{1,2,0:T(4,128)} %param.21) | copy-start | bytes 6148
  3.6 48.8 %copy-start.4 = (bf16[1,128,2048]{2,1,0:T(8,128)(2,1)S(1)}, bf16[1,128,2048]{2,1,0:T(8,128)(2,1)}, u32[]{:S(2)}) copy-start(bf16[1,128,2048]{2,1,0:T(8,128)(2,1)} %stream_ref.1) | copy-start | bytes 1572868
  3.6 48.8 %copy-start.10 = (f32[2048]{0:T(1024)S(1)}, f32[2048]{0:T(1024)}, u32[]{:S(2)}) copy-start(f32[2048]{0:T(1024)} %param.19) | copy-start | bytes 24580
  39.2 13.2 %all-to-all-start.1 = ((bf16[16,128,128]{2,1,0:T(8,128)(2,1)}), bf16[16,128,128]{2,1,0:T(8,128)(2,1)S(1)}, u32[]{:S(2)}, u32[]{:S(2)}) async-start(bf16[16,128,128]{2,1,0:T(8,128)(2,1)} %shard_map.128), calls=%async_computation.1 | async-start | bytes 1048576 | tf_op jit(solution)/shard_map/all_to_all | solution.py:271
  52.4 3.4 %copy-start = (bf16[2048,2048]{1,0:T(8,128)(2,1)S(1)}, bf16[2048,2048]{1,0:T(8,128)(2,1)}, u32[]{:S(2)}) copy-start(bf16[2048,2048]{1,0:T(8,128)(2,1)} %weight_ref.1) | copy-start | bytes 25165828
  58.3 49.3 %copy-start.1 = (bf16[1,2048,512]{2,1,0:T(8,128)(2,1)S(1)}, bf16[1,2048,512]{2,1,0:T(8,128)(2,1)}, u32[]{:S(2)}) copy-start(bf16[1,2048,512]{2,1,0:T(8,128)(2,1)} %gate_ref.1) | copy-start | bytes 6291460
  58.3 49.3 %copy-start.2 = (bf16[1,2048,512]{2,1,0:T(8,128)(2,1)S(1)}, bf16[1,2048,512]{2,1,0:T(8,128)(2,1)}, u32[]{:S(2)}) copy-start(bf16[1,2048,512]{2,1,0:T(8,128)(2,1)} %up_ref.1) | copy-start | bytes 6291460
  58.3 49.2 %copy-start.3 = (bf16[1,512,2048]{2,1,0:T(8,128)(2,1)S(1)}, bf16[1,512,2048]{2,1,0:T(8,128)(2,1)}, u32[]{:S(2)}) copy-start(bf16[1,512,2048]{2,1,0:T(8,128)(2,1)} %down_ref.1) | copy-start | bytes 6291460
  117.4 45.6 %copy-start.9 = (f32[2048]{0:T(1024)S(1)}, f32[2048]{0:T(1024)}, u32[]{:S(2)}) copy-start(f32[2048]{0:T(1024)} %param.25) | copy-start | bytes 24580

commit v2 on v1

--- a/solution.py
+++ b/solution.py
@@ -44,27 +44,96 @@
     return centred * lax.rsqrt(spread + norm_eps) * gain_row
 
 
-def pack_heads_body(q_ref, k_ref, v_ref, out_ref):
+def in_hbm(*arrays):
+    return tuple(pltpu.with_memory_space_constraint(a, pltpu.HBM) for a in arrays)
+
+
+def slot_of(place, kind):
+    if kind == 0:
+        return jnp.where(place < SLOTS, place, -2)
+    return jnp.where(place >= SLOTS, place - SLOTS + 2 * (kind - 1), -2)
+
+
+def prepare_body(
+    q_ref, k_ref, v_ref, ids_hbm, score_hbm, out_ref, pick_ref, blend_ref, ids_ref, score_ref, sems, small
+):
+    lists = [
+        pltpu.make_async_copy(ids_hbm, ids_ref, small.at[0]),
+        pltpu.make_async_copy(score_hbm, score_ref, small.at[1]),
+    ]
+    copies = []
     for h in range(out_ref.shape[0]):
         for n, ref in enumerate((q_ref, k_ref, v_ref)):
-            out_ref[h, n] = ref[0, :, h * LANE : (h + 1) * LANE]
-
-
-def pack_heads(q, k, v):
+            source = ref.at[0, :, h * LANE : (h + 1) * LANE]
+            copies.append(pltpu.make_async_copy(source, out_ref.at[h, n], sems.at[h, n]))
+    for copy in lists + copies:
+        copy.start()
+    for copy in lists:
+        copy.wait()
+    top_k, rows = ids_ref.shape[1:]
+    experts = pick_ref.shape[1] // SUB
+    expert = lax.broadcasted_iota(jnp.int32, (experts, rows), 0)
+    scores = score_ref[0]
+    raised = jnp.exp(scores - jnp.max(scores, axis=0, keepdims=True))
+    shares = raised / jnp.sum(raised, axis=0, keepdims=True)
+    named = jnp.zeros((experts, rows), jnp.float32)
+    share = jnp.zeros((experts, rows), jnp.float32)
+    for k in range(top_k):
+        hit = ids_ref[0, k : k + 1] == expert
+        named = jnp.where(hit, 1.0, named)
+        share = jnp.where(hit, shares[k : k + 1], share)
+    earlier = lax.broadcasted_iota(jnp.int32, (rows, rows), 0) < lax.broadcasted_iota(
+        jnp.int32, (rows, rows), 1
+    )
+    rank = dot(named.astype(jnp.bfloat16), jnp.where(earlier, 1.0, 0.0).astype(jnp.bfloat16))
+    slot = jnp.where(named > 0.0, rank, -1.0)
+    by_expert = jnp.broadcast_to(slot[:, None, :], (experts, SUB, rows))
+    place = lax.broadcasted_iota(jnp.int32, (experts, SUB, rows), 1)
+    for kind in range(4):
+        hit = by_expert == slot_of(place, kind).astype(jnp.float32)
+        pick = jnp.where(hit, 1.0, 0.0).reshape(experts * SUB, rows).astype(jnp.bfloat16)
+        pick_ref[kind] = pick
+    wide = (experts, experts * SUB)
+    spread = lax.broadcasted_iota(jnp.int32, wide, 0) == lax.broadcasted_iota(
+        jnp.int32, wide, 1
+    ) // SUB
+    spread = jnp.where(spread, 1.0, 0.0).astype(jnp.bfloat16)
+    wide_slot = dot(slot.T.astype(jnp.bfloat16), spread)
+    wide_share = dot(share.T.astype(jnp.bfloat16), spread)
+    place = lax.broadcasted_iota(jnp.int32, wide_slot.shape, 1) % SUB
+    for kind in range(4):
+        hit = wide_slot == slot_of(place, kind).astype(jnp.float32)
+        blend_ref[kind] = jnp.where(hit, wide_share, 0.0).astype(jnp.bfloat16)
+    for copy in copies:
+        copy.wait()
+
+
+def prepare(q, k, v, ids, scores, experts):
     rows, width = q.shape[1:]
-    heads, step = width // LANE, 4
-    spec = pl.BlockSpec((1, rows, step * LANE), lambda i: (0, 0, i))
-    return call(
-        pack_heads_body,
-        jax.ShapeDtypeStruct((heads, 3, rows, LANE), q.dtype),
+    heads = width // LANE
+    near = pl.BlockSpec(memory_space=pltpu.VMEM)
+    return call(
+        prepare_body,
+        (
+            pltpu.VMEM((heads, 3, rows, LANE), q.dtype),
+            jax.ShapeDtypeStruct((4, experts * SUB, rows), jnp.bfloat16),
+            jax.ShapeDtypeStruct((4, rows, experts * SUB), jnp.bfloat16),
+        ),
         16,
-        grid=(heads // step,),
-        in_specs=[spec] * 3,
-        out_specs=pl.BlockSpec((step, 3, rows, LANE), lambda i: (i, 0, 0, 0)),
-    )(q, k, v)
-
-
-def attend_body(qkv_ref, gate_ref, out_ref, score_ref):
+        in_specs=[pl.BlockSpec(memory_space=pltpu.HBM)] * 5,
+        out_specs=(near,) * 3,
+        scratch_shapes=[
+            pltpu.VMEM(ids.shape, ids.dtype),
+            pltpu.VMEM(scores.shape, scores.dtype),
+            pltpu.SemaphoreType.DMA((heads, 3)),
+            pltpu.SemaphoreType.DMA((2,)),
+        ],
+    )(*in_hbm(q, k, v, ids, scores))
+
+
+def attend_body(qkv_ref, gate_ref, weight_ref, out_ref, near_ref, score_ref, sem):
+    brought = pltpu.make_async_copy(weight_ref, near_ref, sem)
+    brought.start()
     parts, _, rows, size = qkv_ref.shape
     pair = 2
     block = pair * rows
@@ -96,71 +165,26 @@
         row_total = jnp.sum(total, axis=1, keepdims=True)
         done = (blended / row_total).astype(jnp.bfloat16)
         out_ref[pair * b : pair * (b + 1)] = done.reshape(pair, rows, size)
-
-
-def attend(qkv, gates):
+    brought.wait()
+
+
+def attend(qkv, gates, weight):
     parts, _, rows, size = qkv.shape
+    near = pl.BlockSpec(memory_space=pltpu.VMEM)
     return call(
         attend_body,
-        jax.ShapeDtypeStruct((parts, rows, size), qkv.dtype),
-        24,
-        scratch_shapes=[pltpu.VMEM((2 * rows, parts * rows), jnp.float32)],
-    )(qkv, gates)
-
-
-def slot_of(place, kind):
-    if kind == 0:
-        return jnp.where(place < SLOTS, place, -2)
-    return jnp.where(place >= SLOTS, place - SLOTS + 2 * (kind - 1), -2)
-
-
-def route_body(ids_ref, score_ref, pick_ref, blend_ref):
-    rows, top_k = ids_ref.shape[1:]
-    experts = pick_ref.shape[1] // SUB
-    expert = lax.broadcasted_iota(jnp.int32, (rows, experts), 1)
-    scores = score_ref[0]
-    raised = jnp.exp(scores - jnp.max(scores, axis=1, keepdims=True))
-    shares = raised / jnp.sum(raised, axis=1, keepdims=True)
-    named = jnp.zeros((rows, experts), jnp.float32)
-    share = jnp.zeros((rows, experts), jnp.float32)
-    for k in range(top_k):
-        hit = ids_ref[0, :, k : k + 1] == expert
-        named = jnp.where(hit, 1.0, named)
-        share = jnp.where(hit, shares[:, k : k + 1], share)
-    earlier = lax.broadcasted_iota(jnp.int32, (rows, rows), 0) > lax.broadcasted_iota(
-        jnp.int32, (rows, rows), 1
-    )
-    rank = dot(jnp.where(earlier, 1.0, 0.0).astype(jnp.bfloat16), named.astype(jnp.bfloat16))
-    slot = jnp.where(named > 0.0, rank, -1.0)
-    by_expert = jnp.broadcast_to(slot.T[:, None, :], (experts, SUB, rows))
-    place = lax.broadcasted_iota(jnp.int32, (experts, SUB, rows), 1)
-    for kind in range(4):
-        hit = by_expert == slot_of(place, kind).astype(jnp.float32)
-        pick = jnp.where(hit, 1.0, 0.0).reshape(experts * SUB, rows).astype(jnp.bfloat16)
-        pick_ref[kind] = pick
-    wide = (experts, experts * SUB)
-    spread = lax.broadcasted_iota(jnp.int32, wide, 0) == lax.broadcasted_iota(
-        jnp.int32, wide, 1
-    ) // SUB
-    spread = jnp.where(spread, 1.0, 0.0).astype(jnp.bfloat16)
-    wide_slot = dot(slot.astype(jnp.bfloat16), spread)
-    wide_share = dot(share.astype(jnp.bfloat16), spread)
-    place = lax.broadcasted_iota(jnp.int32, wide_slot.shape, 1) % SUB
-    for kind in range(4):
-        hit = wide_slot == slot_of(place, kind).astype(jnp.float32)
-        blend_ref[kind] = jnp.where(hit, wide_share, 0.0).astype(jnp.bfloat16)
-
-
-def route(ids, scores, experts):
-    rows = ids.shape[1]
-    return call(
-        route_body,
         (
-            jax.ShapeDtypeStruct((4, experts * SUB, rows), jnp.bfloat16),
-            jax.ShapeDtypeStruct((4, rows, experts * SUB), jnp.bfloat16),
+            jax.ShapeDtypeStruct((parts, rows, size), qkv.dtype),
+            pltpu.VMEM(weight.shape, weight.dtype),
         ),
-        24,
-    )(ids, scores)
+        20,
+        in_specs=[near, near, pl.BlockSpec(memory_space=pltpu.HBM)],
+        out_specs=(near, near),
+        scratch_shapes=[
+            pltpu.VMEM((2 * rows, parts * rows), jnp.float32),
+            pltpu.SemaphoreType.DMA,
+        ],
+    )(qkv, gates, *in_hbm(weight))
 
 
 def project_body(heads_ref, stream_ref, weight_ref, gain_ref, pick_ref, first_ref, out_ref):
@@ -195,41 +219,33 @@
     )(heads, stream, weight, gain, pick)
 
 
-def move_matrix(rows, p):
-    to = lax.broadcasted_iota(jnp.int32, (rows, rows), 0)
-    fro = lax.broadcasted_iota(jnp.int32, (rows, rows), 1)
-    same = to // SUB == fro // SUB
-    hit = same & (fro % SUB - SLOTS + 2 * p == to % SUB) & (fro % SUB >= SLOTS)
-    return jnp.where(hit, 1.0, 0.0).astype(jnp.bfloat16)
-
-
 def expert_body(in_ref, gate_ref, up_ref, down_ref, out_ref):
     sources = in_ref.shape[0]
     rows = sources * SUB
+    place = lax.broadcasted_iota(jnp.int32, (rows, LANE), 0) % SUB
     kept = [in_ref[:, t].reshape(rows, LANE) for t in range(MAIN)]
-    tail = jnp.zeros((rows, TAIL * LANE), jnp.float32)
-    for p in range(3):
-        spare = jnp.concatenate([kept[3 * q + p] for q in range(TAIL)], axis=1)
-        tail = tail + dot(move_matrix(rows, p), spare)
-    x = jnp.concatenate(kept + [tail.astype(jnp.bfloat16)], axis=1)
+    tail = []
+    for q in range(TAIL):
+        spare = [
+            pltpu.roll(kept[3 * q + p].astype(jnp.float32), rows - SLOTS + 2 * p, 0)
+            for p in range(3)
+        ]
+        block = jnp.where(place < 2, spare[0], jnp.where(place < 4, spare[1], spare[2]))
+        tail.append(block.astype(jnp.bfloat16))
+    x = jnp.concatenate(kept + tail, axis=1)
     gate_act = jnp.minimum(dot(x, gate_ref[0]), clamp_limit)
     up_act = jnp.clip(dot(x, up_ref[0]), -clamp_limit, clamp_limit)
     hidden = gate_act * jax.nn.sigmoid(swish_alpha * gate_act) * (up_act + 1.0)
     y = dot(hidden.astype(jnp.bfloat16), down_ref[0])
-    y_tail = y[:, MAIN * LANE :].astype(jnp.bfloat16)
-    own = lax.broadcasted_iota(jnp.int32, (rows, LANE), 0) % SUB < SLOTS
-    for p in range(3):
-        spare = dot(move_matrix(rows, p), y_tail, ((0,), (0,)))
-        for q in range(TAIL):
-            t = 3 * q + p
-            tile = jnp.where(
-                own, y[:, t * LANE : (t + 1) * LANE], spare[:, q * LANE : (q + 1) * LANE]
-            )
-            out_ref[:, t] = tile.astype(jnp.bfloat16).reshape(sources, SUB, LANE)
+    for t in range(MAIN):
+        q, p = t // 3, t % 3
+        spare = pltpu.roll(y[:, (MAIN + q) * LANE : (MAIN + q + 1) * LANE], SLOTS - 2 * p, 0)
+        tile = jnp.where(place < SLOTS, y[:, t * LANE : (t + 1) * LANE], spare)
+        out_ref[:, t] = tile.astype(jnp.bfloat16).reshape(sources, SUB, LANE)
 
 
 def expert(arrived, gate, up, down):
-    sources, step = arrived.shape[0], 32
+    sources, step = arrived.shape[0], 64
     block = pl.BlockSpec((step, MAIN, SUB, LANE), lambda i: (i, 0, 0, 0))
     whole = [pl.BlockSpec(w.shape, lambda i: (0, 0, 0)) for w in (gate, up, down)]
     return call(
@@ -287,10 +303,18 @@
     second_gain,
 ):
     experts = lax.axis_size(SP_DP)
-    qkv = exchange(pack_heads(query_rows, key_rows, value_rows), SP)
-    pick, blend = route(expert_ids, route_scores, experts)
-    heads = exchange(attend(qkv, forget_sums[0]), SP)
-    first, outgoing = project(heads, stream, out_weight, first_gain[None], pick)
+    packed, pick, blend = prepare(
+        query_rows,
+        key_rows,
+        value_rows,
+        expert_ids.transpose(0, 2, 1),
+        route_scores.transpose(0, 2, 1),
+        experts,
+    )
+    qkv = exchange(packed, SP)
+    attended, near_weight = attend(qkv, forget_sums[0], out_weight)
+    heads = exchange(attended, SP)
+    first, outgoing = project(heads, stream, near_weight, first_gain[None], pick)
     arrived = exchange(outgoing, SP_DP)
     finished = expert(arrived, gate_weight, up_weight, down_weight)
     returned = exchange(finished, SP_DP)

time: 166 us -> 158 us (0.952)
  blocking collectives: 125 us -> 138 us
  waiting for transfers between devices: 8.45 us -> 0 us
  local copies, waits for them, and re-layouts: 6.79 us -> 0.04 us
  starting transfers between devices: 3.57 us -> 0 us
    all_to_all x3 -> x4, blocking collectives: 125 us -> 138 us  [exchange(): return lax.all_to_all(x, axes, split_axis=0, concat_axis=0, tiled=True)]
    all_to_all x1 -> x0, waiting for transfers between devices: 8.45 us -> none  [exchange(): return lax.all_to_all(x, axes, split_axis=0, concat_axis=0, tiled=True)]
    unnamed x28 -> x14, local copies, waits for them, and re-layouts: 6.79 us -> 0.04 us
    all_to_all x1 -> x0, starting transfers between devices: 3.57 us -> none  [exchange(): return lax.all_to_all(x, axes, split_axis=0, concat_axis=0, tiled=True)]
    pallas_call x1, Pallas kernels: 9.83 us -> 8.01 us  [expert(): call(expert_body, jax.ShapeDtypeStruct(arrived.shape, arrived.dtype), 36,...]
    pallas_call x3 -> x2, Pallas kernels: 6.74 us -> 7.17 us  [the longest x1 4.61 us: attend(): call(attend_body, (jax.ShapeDtypeStruct((parts, rows, size), qkv.dtype),...]
  transfers between devices with their start and end apart: 1 -> 0, of which waited for: 1 -> 0; matrix products, arithmetic and copies ran while one was open for 0% -> 0% of each run, Pallas kernels for 1% -> 0%
where the time goes in v2:
time: 158 us
  blocking collectives  138 us (87%)
  Pallas kernels  19.8 us (13%)
    all_to_all x4, blocking collectives, exchange(): return lax.all_to_all(x, axes, split_axis=0, concat_axis=0, tiled=True)  138 us
    pallas_call x1, Pallas kernels, expert(): call(expert_body, jax.ShapeDtypeStruct(arrived.shape, arrived.dtype), 36,...  8.01 us
    pallas_call x1, Pallas kernels, attend(): call(attend_body, (jax.ShapeDtypeStruct((parts, rows, size), qkv.dtype),...  4.61 us

profile of v2, /device:TPU:1, one launch (start us, length us, event | category | flops | bytes accessed | tf_op | source)
XLA Modules:
  0.0 157.7 jit_solution(34120975318481452)
XLA Ops:
  0.0 0.0 copy-start.5
  0.0 2.6 %shard_map.127 = (bf16[16,3,128,128]{3,2,1,0:T(8,128)(2,1)S(1)}, bf16[4,1024,128]{2,1,0:T(8,128)(2,1)S(1)}, bf16[4,128,1024]{2,1,0:T(8,128)(2,1)S(1)}) custom-call(bf16[1,128,2048]{2,1,0:T(8,128)(2,1)} %q_ref.1, bf16[1,128,2048]{2,1,0:T(8,128)(2,1)} %k_ref.1, bf16[1,128,2048]{2,1,0:T(8,128)(2,1)} %v_ref.1, s32[1,4,128]{2,1,0:T(4,128)} %bitcast.8, ...), custom_call_target="tpu_custom_call" | custom-call | tf_op jit(solution)/shard_map/pallas_call | solution.py:115
  2.6 30.0 %all_to_all.20.qkv_ref = bf16[16,3,128,128]{3,2,1,0:T(8,128)(2,1)S(1)} all-to-all(bf16[16,3,128,128]{3,2,1,0:T(8,128)(2,1)S(1)} %get-tuple-element.12), channel_id=1, replica_groups=mesh['sp_0'=4,'sp_1'=4,'dp'=8] {'sp_0','sp_1'}, dimensions={0} | all-to-all | bytes 3145728 | tf_op jit(solution)/shard_map/all_to_all | solution.py:287
  32.6 0.0 copy-done.5
  32.6 0.0 copy-start.3
  32.6 0.0 copy-start.6
  32.6 4.6 %shard_map.128 = (bf16[16,128,128]{2,1,0:T(8,128)(2,1)S(1)}, bf16[2048,2048]{1,0:T(8,128)(2,1)S(1)}) custom-call(bf16[16,3,128,128]{3,2,1,0:T(8,128)(2,1)S(1)} %all_to_all.20.qkv_ref, f32[1,2048]{1,0:T(1,128)S(1)} %bitcast.6, bf16[2048,2048]{1,0:T(8,128)(2,1)} %weight_ref.1), custom_call_target="tpu_custom_call" | custom-call | tf_op jit(solution)/shard_map/pallas_call | solution.py:174
  37.2 13.4 %all_to_all.21.heads_ref = bf16[16,128,128]{2,1,0:T(8,128)(2,1)S(1)} all-to-all(bf16[16,128,128]{2,1,0:T(8,128)(2,1)S(1)} %get-tuple-element.13), channel_id=1, replica_groups=mesh['sp_0'=4,'sp_1'=4,'dp'=8] {'sp_0','sp_1'}, dimensions={0} | all-to-all | bytes 1048576 | tf_op jit(solution)/shard_map/all_to_all | solution.py:287
  50.6 0.0 copy-done.3
  50.6 0.0 copy-done.6
  50.6 2.5 %shard_map.129 = (bf16[128,2048]{1,0:T(8,128)(2,1)S(1)}, bf16[128,12,8,128]{3,2,1,0:T(8,128)(2,1)S(1)}) custom-call(bf16[16,128,128]{2,1,0:T(8,128)(2,1)S(1)} %all_to_all.21.heads_ref, bf16[1,128,2048]{2,1,0:T(8,128)(2,1)S(1)} %copy-done.3, bf16[2048,2048]{1,0:T(8,128)(2,1)S(1)} %get-tuple-element.14.weight_ref, f32[1,2048]{1,0:T(1,128)S(1)} %bitcast.7, ...), custom_call_target="tpu_custom_call" | custom-call | tf_op jit(solution)/shard_map/pallas_call | solution.py:212
  53.2 0.0 copy-start
  53.2 0.0 copy-start.1
  53.2 0.0 copy-start.2
  53.2 48.7 %all_to_all.22.in_ref = bf16[128,12,8,128]{3,2,1,0:T(8,128)(2,1)S(1)} all-to-all(bf16[128,12,8,128]{3,2,1,0:T(8,128)(2,1)S(1)} %get-tuple-element.16), channel_id=1, replica_groups=mesh['sp_0'=4,'sp_1'=4,'dp'=8] {'sp_0','sp_1','dp'}, dimensions={0} | all-to-all | bytes 6291456 | tf_op jit(solution)/shard_map/all_to_all | solution.py:287
  101.9 0.0 copy-done
  101.9 0.0 copy-done.1
  101.9 0.0 copy-done.2
  101.9 8.0 %shard_map.130 = bf16[128,12,8,128]{3,2,1,0:T(8,128)(2,1)S(1)} custom-call(bf16[128,12,8,128]{3,2,1,0:T(8,128)(2,1)S(1)} %all_to_all.22.in_ref, bf16[1,2048,512]{2,1,0:T(8,128)(2,1)S(1)} %copy-done, bf16[1,2048,512]{2,1,0:T(8,128)(2,1)S(1)} %copy-done.1, bf16[1,512,2048]{2,1,0:T(8,128)(2,1)S(1)} %copy-done.2), custom_call_target="tpu_custom_call" | custom-call | tf_op jit(solution)/shard_map/pallas_call | solution.py:251
  110.0 0.0 copy-start.4
  110.0 45.6 %all_to_all.23.in_ref = bf16[128,12,8,128]{3,2,1,0:T(8,128)(2,1)S(1)} all-to-all(bf16[128,12,8,128]{3,2,1,0:T(8,128)(2,1)S(1)} %shard_map.130), channel_id=1, replica_groups=mesh['sp_0'=4,'sp_1'=4,'dp'=8] {'sp_0','sp_1','dp'}, dimensions={0} | all-to-all | bytes 6291456 | tf_op jit(solution)/shard_map/all_to_all | solution.py:287
  155.6 0.0 copy-done.4
  155.6 2.1 %shard_map.131 = bf16[1,128,2048]{2,1,0:T(8,128)(2,1)} custom-call(bf16[128,12,8,128]{3,2,1,0:T(8,128)(2,1)S(1)} %all_to_all.23.in_ref, bf16[4,128,1024]{2,1,0:T(8,128)(2,1)S(1)} %get-tuple-element.17.blend_ref, bf16[128,2048]{1,0:T(8,128)(2,1)S(1)} %get-tuple-element.18.first_ref, f32[1,2048]{1,0:T(1,128)S(1)} %bitcast.5), custom_call_target="tpu_custom_call" | custom-call | tf_op jit(solution)/shard_map/pallas_call | solution.py:279
Async XLA Ops:
  0.0 32.6 %copy-start.5 = (f32[1,1,2048]{2,1,0:T(1,128)S(1)}, f32[1,1,2048]{2,1,0:T(1,128)}, u32[]{:S(2)}) copy-start(f32[1,1,2048]{2,1,0:T(1,128)} %param.17) | copy-start | bytes 24580
  32.6 18.0 %copy-start.3 = (bf16[1,128,2048]{2,1,0:T(8,128)(2,1)S(1)}, bf16[1,128,2048]{2,1,0:T(8,128)(2,1)}, u32[]{:S(2)}) copy-start(bf16[1,128,2048]{2,1,0:T(8,128)(2,1)} %stream_ref.1) | copy-start | bytes 1572868
  32.6 18.0 %copy-start.6 = (f32[2048]{0:T(1024)S(1)}, f32[2048]{0:T(1024)}, u32[]{:S(2)}) copy-start(f32[2048]{0:T(1024)} %param.19) | copy-start | bytes 24580
  53.2 48.8 %copy-start = (bf16[1,2048,512]{2,1,0:T(8,128)(2,1)S(1)}, bf16[1,2048,512]{2,1,0:T(8,128)(2,1)}, u32[]{:S(2)}) copy-start(bf16[1,2048,512]{2,1,0:T(8,128)(2,1)} %gate_ref.1) | copy-start | bytes 6291460
  53.2 48.8 %copy-start.1 = (bf16[1,2048,512]{2,1,0:T(8,128)(2,1)S(1)}, bf16[1,2048,512]{2,1,0:T(8,128)(2,1)}, u32[]{:S(2)}) copy-start(bf16[1,2048,512]{2,1,0:T(8,128)(2,1)} %up_ref.1) | copy-start | bytes 6291460
  53.2 48.8 %copy-start.2 = (bf16[1,512,2048]{2,1,0:T(8,128)(2,1)S(1)}, bf16[1,512,2048]{2,1,0:T(8,128)(2,1)}, u32[]{:S(2)}) copy-start(bf16[1,512,2048]{2,1,0:T(8,128)(2,1)} %down_ref.1) | copy-start | bytes 6291460
  110.0 45.6 %copy-start.4 = (f32[2048]{0:T(1024)S(1)}, f32[2048]{0:T(1024)}, u32[]{:S(2)}) copy-start(f32[2048]{0:T(1024)} %param.25) | copy-start | bytes 24580

commit v3 on v2

--- a/solution.py
+++ b/solution.py
@@ -55,17 +55,28 @@
 
 
 def prepare_body(
-    q_ref, k_ref, v_ref, ids_hbm, score_hbm, out_ref, pick_ref, blend_ref, ids_ref, score_ref, sems, small
+    q_ref,
+    k_ref,
+    v_ref,
+    ids_hbm,
+    score_hbm,
+    out_ref,
+    pick_ref,
+    blend_ref,
+    ids_ref,
+    score_ref,
+    land_ref,
+    sems,
+    small,
 ):
     lists = [
         pltpu.make_async_copy(ids_hbm, ids_ref, small.at[0]),
         pltpu.make_async_copy(score_hbm, score_ref, small.at[1]),
     ]
-    copies = []
-    for h in range(out_ref.shape[0]):
-        for n, ref in enumerate((q_ref, k_ref, v_ref)):
-            source = ref.at[0, :, h * LANE : (h + 1) * LANE]
-            copies.append(pltpu.make_async_copy(source, out_ref.at[h, n], sems.at[h, n]))
+    copies = [
+        pltpu.make_async_copy(ref.at[0], land_ref.at[n], sems.at[n])
+        for n, ref in enumerate((q_ref, k_ref, v_ref))
+    ]
     for copy in lists + copies:
         copy.start()
     for copy in lists:
@@ -104,8 +115,10 @@
     for kind in range(4):
         hit = wide_slot == slot_of(place, kind).astype(jnp.float32)
         blend_ref[kind] = jnp.where(hit, wide_share, 0.0).astype(jnp.bfloat16)
-    for copy in copies:
+    for n, copy in enumerate(copies):
         copy.wait()
+        for h in range(out_ref.shape[0]):
+            out_ref[h, n] = land_ref[n, :, h * LANE : (h + 1) * LANE]
 
 
 def prepare(q, k, v, ids, scores, experts):
@@ -125,7 +138,8 @@
         scratch_shapes=[
             pltpu.VMEM(ids.shape, ids.dtype),
             pltpu.VMEM(scores.shape, scores.dtype),
-            pltpu.SemaphoreType.DMA((heads, 3)),
+            pltpu.VMEM((3, rows, width), q.dtype),
+            pltpu.SemaphoreType.DMA((3,)),
             pltpu.SemaphoreType.DMA((2,)),
         ],
     )(*in_hbm(q, k, v, ids, scores))
@@ -138,33 +152,44 @@
     pair = 2
     block = pair * rows
     scale = size ** (-0.5) * log2_e
-    for b in range(parts // pair):
-        q = qkv_ref[pair * b : pair * (b + 1), 0].reshape(block, size)
+
+    def part(j, n):
+        return qkv_ref[pair * j : pair * (j + 1), n].reshape(block, size)
+
+    def score_rows(b):
+        q = part(b, 0)
         base = gate_ref[:, block * b : block * b + 1]
         top = jnp.full((block, LANE), mask_fill, jnp.float32)
         for j in range(b + 1):
-            keys = qkv_ref[pair * j : pair * (j + 1), 1].reshape(block, size)
             bias = (gate_ref[:, block * j : block * (j + 1)] - base) * log2_e
-            s = dot(q, keys, ((1,), (1,))) * scale - bias
+            s = dot(q, part(j, 1), ((1,), (1,))) * scale - bias
             if j == b:
                 row = lax.broadcasted_iota(jnp.int32, s.shape, 0)
                 col = lax.broadcasted_iota(jnp.int32, s.shape, 1)
                 s = jnp.where(row >= col, s, mask_fill)
-            score_ref[:, block * j : block * (j + 1)] = s
+            score_ref[b % 2, :, block * j : block * (j + 1)] = s
             for c in range(block // LANE):
                 top = jnp.maximum(top, s[:, c * LANE : (c + 1) * LANE])
-        row_max = jnp.max(top, axis=1, keepdims=True)
+        return jnp.max(top, axis=1, keepdims=True)
+
+    def blend_rows(b, row_max):
         total = jnp.zeros((block, LANE), jnp.float32)
         blended = jnp.zeros((block, size), jnp.float32)
         for j in range(b + 1):
-            w = jnp.exp2(score_ref[:, block * j : block * (j + 1)] - row_max)
+            w = jnp.exp2(score_ref[b % 2, :, block * j : block * (j + 1)] - row_max)
             for c in range(block // LANE):
                 total = total + w[:, c * LANE : (c + 1) * LANE]
-            values = qkv_ref[pair * j : pair * (j + 1), 2].reshape(block, size)
-            blended = blended + dot(w.astype(jnp.bfloat16), values)
+            blended = blended + dot(w.astype(jnp.bfloat16), part(j, 2))
         row_total = jnp.sum(total, axis=1, keepdims=True)
         done = (blended / row_total).astype(jnp.bfloat16)
         out_ref[pair * b : pair * (b + 1)] = done.reshape(pair, rows, size)
+
+    count = parts // pair
+    row_max = score_rows(0)
+    for b in range(count):
+        ahead = score_rows(b + 1) if b + 1 < count else None
+        blend_rows(b, row_max)
+        row_max = ahead
     brought.wait()
 
 
@@ -181,7 +206,7 @@
         in_specs=[near, near, pl.BlockSpec(memory_space=pltpu.HBM)],
         out_specs=(near, near),
         scratch_shapes=[
-            pltpu.VMEM((2 * rows, parts * rows), jnp.float32),
+            pltpu.VMEM((2, 2 * rows, parts * rows), jnp.float32),
             pltpu.SemaphoreType.DMA,
         ],
     )(qkv, gates, *in_hbm(weight))
@@ -233,15 +258,24 @@
         block = jnp.where(place < 2, spare[0], jnp.where(place < 4, spare[1], spare[2]))
         tail.append(block.astype(jnp.bfloat16))
     x = jnp.concatenate(kept + tail, axis=1)
-    gate_act = jnp.minimum(dot(x, gate_ref[0]), clamp_limit)
-    up_act = jnp.clip(dot(x, up_ref[0]), -clamp_limit, clamp_limit)
-    hidden = gate_act * jax.nn.sigmoid(swish_alpha * gate_act) * (up_act + 1.0)
-    y = dot(hidden.astype(jnp.bfloat16), down_ref[0])
-    for t in range(MAIN):
-        q, p = t // 3, t % 3
-        spare = pltpu.roll(y[:, (MAIN + q) * LANE : (MAIN + q + 1) * LANE], SLOTS - 2 * p, 0)
-        tile = jnp.where(place < SLOTS, y[:, t * LANE : (t + 1) * LANE], spare)
-        out_ref[:, t] = tile.astype(jnp.bfloat16).reshape(sources, SUB, LANE)
+    hidden = []
+    units = gate_ref.shape[2]
+    for lo in range(0, units, units // 2):
+        half = slice(lo, lo + units // 2)
+        gate_act = jnp.minimum(dot(x, gate_ref[0, :, half]), clamp_limit)
+        up_act = jnp.clip(dot(x, up_ref[0, :, half]), -clamp_limit, clamp_limit)
+        act = gate_act * jax.nn.sigmoid(swish_alpha * gate_act) * (up_act + 1.0)
+        hidden.append(act.astype(jnp.bfloat16))
+    hidden = jnp.concatenate(hidden, axis=1)
+    y_tail = dot(hidden, down_ref[0, :, MAIN * LANE :])
+    for first in range(0, MAIN, TAIL):
+        y = dot(hidden, down_ref[0, :, first * LANE : (first + TAIL) * LANE])
+        for i in range(TAIL):
+            t = first + i
+            q, p = t // 3, t % 3
+            spare = pltpu.roll(y_tail[:, q * LANE : (q + 1) * LANE], SLOTS - 2 * p, 0)
+            tile = jnp.where(place < SLOTS, y[:, i * LANE : (i + 1) * LANE], spare)
+            out_ref[:, t] = tile.astype(jnp.bfloat16).reshape(sources, SUB, LANE)
 
 
 def expert(arrived, gate, up, down):

time: 158 us -> 156 us (0.987)
  Pallas kernels: 19.8 us -> 17.5 us
where the time goes in v3:
time: 156 us; the launch traced here: 155 us
  blocking collectives  138 us (88%)
  Pallas kernels  17.5 us (11%)
    all_to_all x4, blocking collectives, exchange(): return lax.all_to_all(x, axes, split_axis=0, concat_axis=0, tiled=True)  138 us
    pallas_call x1, Pallas kernels, expert(): call(expert_body, jax.ShapeDtypeStruct(arrived.shape, arrived.dtype), 36,...  7.23 us
    pallas_call x1, Pallas kernels, attend(): call(attend_body, (jax.ShapeDtypeStruct((parts, rows, size), qkv.dtype),...  3.53 us

profile of v3, /device:TPU:1, one launch (start us, length us, event | category | flops | bytes accessed | tf_op | source)
XLA Modules:
  0.0 155.4 jit_solution(15524204013680616440)
XLA Ops:
  0.0 0.0 copy-start.5
  0.0 2.1 %shard_map.127 = (bf16[16,3,128,128]{3,2,1,0:T(8,128)(2,1)S(1)}, bf16[4,1024,128]{2,1,0:T(8,128)(2,1)S(1)}, bf16[4,128,1024]{2,1,0:T(8,128)(2,1)S(1)}) custom-call(bf16[1,128,2048]{2,1,0:T(8,128)(2,1)} %q_ref.1, bf16[1,128,2048]{2,1,0:T(8,128)(2,1)} %k_ref.1, bf16[1,128,2048]{2,1,0:T(8,128)(2,1)} %v_ref.1, s32[1,4,128]{2,1,0:T(4,128)} %bitcast.8, ...), custom_call_target="tpu_custom_call" | custom-call | tf_op jit(solution)/shard_map/pallas_call | solution.py:128
  2.1 30.0 %all_to_all.20.qkv_ref = bf16[16,3,128,128]{3,2,1,0:T(8,128)(2,1)S(1)} all-to-all(bf16[16,3,128,128]{3,2,1,0:T(8,128)(2,1)S(1)} %get-tuple-element.12), channel_id=1, replica_groups=mesh['sp_0'=4,'sp_1'=4,'dp'=8] {'sp_0','sp_1'}, dimensions={0} | all-to-all | bytes 3145728 | tf_op jit(solution)/shard_map/all_to_all | solution.py:321
  32.2 0.0 copy-done.5
  32.2 0.0 copy-start.3
  32.2 0.0 copy-start.6
  32.2 3.5 %shard_map.128 = (bf16[16,128,128]{2,1,0:T(8,128)(2,1)S(1)}, bf16[2048,2048]{1,0:T(8,128)(2,1)S(1)}) custom-call(bf16[16,3,128,128]{3,2,1,0:T(8,128)(2,1)S(1)} %all_to_all.20.qkv_ref, f32[1,2048]{1,0:T(1,128)S(1)} %bitcast.6, bf16[2048,2048]{1,0:T(8,128)(2,1)} %weight_ref.1), custom_call_target="tpu_custom_call" | custom-call | tf_op jit(solution)/shard_map/pallas_call | solution.py:199
  35.7 13.4 %all_to_all.21.heads_ref = bf16[16,128,128]{2,1,0:T(8,128)(2,1)S(1)} all-to-all(bf16[16,128,128]{2,1,0:T(8,128)(2,1)S(1)} %get-tuple-element.13), channel_id=1, replica_groups=mesh['sp_0'=4,'sp_1'=4,'dp'=8] {'sp_0','sp_1'}, dimensions={0} | all-to-all | bytes 1048576 | tf_op jit(solution)/shard_map/all_to_all | solution.py:321
  49.1 0.0 copy-done.3
  49.1 0.0 copy-done.6
  49.1 2.5 %shard_map.129 = (bf16[128,2048]{1,0:T(8,128)(2,1)S(1)}, bf16[128,12,8,128]{3,2,1,0:T(8,128)(2,1)S(1)}) custom-call(bf16[16,128,128]{2,1,0:T(8,128)(2,1)S(1)} %all_to_all.21.heads_ref, bf16[1,128,2048]{2,1,0:T(8,128)(2,1)S(1)} %copy-done.3, bf16[2048,2048]{1,0:T(8,128)(2,1)S(1)} %get-tuple-element.14.weight_ref, f32[1,2048]{1,0:T(1,128)S(1)} %bitcast.7, ...), custom_call_target="tpu_custom_call" | custom-call | tf_op jit(solution)/shard_map/pallas_call | solution.py:237
  51.6 0.0 copy-start
  51.6 0.0 copy-start.1
  51.7 0.0 copy-start.2
  51.7 48.7 %all_to_all.22.in_ref = bf16[128,12,8,128]{3,2,1,0:T(8,128)(2,1)S(1)} all-to-all(bf16[128,12,8,128]{3,2,1,0:T(8,128)(2,1)S(1)} %get-tuple-element.16), channel_id=1, replica_groups=mesh['sp_0'=4,'sp_1'=4,'dp'=8] {'sp_0','sp_1','dp'}, dimensions={0} | all-to-all | bytes 6291456 | tf_op jit(solution)/shard_map/all_to_all | solution.py:321
  100.4 0.0 copy-done
  100.4 0.0 copy-done.1
  100.4 0.0 copy-done.2
  100.4 7.2 %shard_map.130 = bf16[128,12,8,128]{3,2,1,0:T(8,128)(2,1)S(1)} custom-call(bf16[128,12,8,128]{3,2,1,0:T(8,128)(2,1)S(1)} %all_to_all.22.in_ref, bf16[1,2048,512]{2,1,0:T(8,128)(2,1)S(1)} %copy-done, bf16[1,2048,512]{2,1,0:T(8,128)(2,1)S(1)} %copy-done.1, bf16[1,512,2048]{2,1,0:T(8,128)(2,1)S(1)} %copy-done.2), custom_call_target="tpu_custom_call" | custom-call | tf_op jit(solution)/shard_map/pallas_call | solution.py:285
  107.7 0.0 copy-start.4
  107.7 45.6 %all_to_all.23.in_ref = bf16[128,12,8,128]{3,2,1,0:T(8,128)(2,1)S(1)} all-to-all(bf16[128,12,8,128]{3,2,1,0:T(8,128)(2,1)S(1)} %shard_map.130), channel_id=1, replica_groups=mesh['sp_0'=4,'sp_1'=4,'dp'=8] {'sp_0','sp_1','dp'}, dimensions={0} | all-to-all | bytes 6291456 | tf_op jit(solution)/shard_map/all_to_all | solution.py:321
  153.3 0.0 copy-done.4
  153.3 2.1 %shard_map.131 = bf16[1,128,2048]{2,1,0:T(8,128)(2,1)} custom-call(bf16[128,12,8,128]{3,2,1,0:T(8,128)(2,1)S(1)} %all_to_all.23.in_ref, bf16[4,128,1024]{2,1,0:T(8,128)(2,1)S(1)} %get-tuple-element.17.blend_ref, bf16[128,2048]{1,0:T(8,128)(2,1)S(1)} %get-tuple-element.18.first_ref, f32[1,2048]{1,0:T(1,128)S(1)} %bitcast.5), custom_call_target="tpu_custom_call" | custom-call | tf_op jit(solution)/shard_map/pallas_call | solution.py:313
Async XLA Ops:
  0.0 32.2 %copy-start.5 = (f32[1,1,2048]{2,1,0:T(1,128)S(1)}, f32[1,1,2048]{2,1,0:T(1,128)}, u32[]{:S(2)}) copy-start(f32[1,1,2048]{2,1,0:T(1,128)} %param.17) | copy-start | bytes 24580
  32.2 16.9 %copy-start.3 = (bf16[1,128,2048]{2,1,0:T(8,128)(2,1)S(1)}, bf16[1,128,2048]{2,1,0:T(8,128)(2,1)}, u32[]{:S(2)}) copy-start(bf16[1,128,2048]{2,1,0:T(8,128)(2,1)} %stream_ref.1) | copy-start | bytes 1572868
  32.2 16.9 %copy-start.6 = (f32[2048]{0:T(1024)S(1)}, f32[2048]{0:T(1024)}, u32[]{:S(2)}) copy-start(f32[2048]{0:T(1024)} %param.19) | copy-start | bytes 24580
  51.6 48.8 %copy-start = (bf16[1,2048,512]{2,1,0:T(8,128)(2,1)S(1)}, bf16[1,2048,512]{2,1,0:T(8,128)(2,1)}, u32[]{:S(2)}) copy-start(bf16[1,2048,512]{2,1,0:T(8,128)(2,1)} %gate_ref.1) | copy-start | bytes 6291460
  51.6 48.8 %copy-start.1 = (bf16[1,2048,512]{2,1,0:T(8,128)(2,1)S(1)}, bf16[1,2048,512]{2,1,0:T(8,128)(2,1)}, u32[]{:S(2)}) copy-start(bf16[1,2048,512]{2,1,0:T(8,128)(2,1)} %up_ref.1) | copy-start | bytes 6291460
  51.7 48.8 %copy-start.2 = (bf16[1,512,2048]{2,1,0:T(8,128)(2,1)S(1)}, bf16[1,512,2048]{2,1,0:T(8,128)(2,1)}, u32[]{:S(2)}) copy-start(bf16[1,512,2048]{2,1,0:T(8,128)(2,1)} %down_ref.1) | copy-start | bytes 6291460
  107.7 45.6 %copy-start.4 = (f32[2048]{0:T(1024)S(1)}, f32[2048]{0:T(1024)}, u32[]{:S(2)}) copy-start(f32[2048]{0:T(1024)} %param.25) | copy-start | bytes 24580

commit v4 on v3

--- a/solution.py
+++ b/solution.py
@@ -184,10 +184,10 @@
         done = (blended / row_total).astype(jnp.bfloat16)
         out_ref[pair * b : pair * (b + 1)] = done.reshape(pair, rows, size)
 
-    count = parts // pair
-    row_max = score_rows(0)
-    for b in range(count):
-        ahead = score_rows(b + 1) if b + 1 < count else None
+    last = parts // pair - 1
+    row_max = score_rows(last)
+    for b in range(last, -1, -1):
+        ahead = score_rows(b - 1) if b > 0 else None
         blend_rows(b, row_max)
         row_max = ahead
     brought.wait()
@@ -245,21 +245,34 @@
 
 
 def expert_body(in_ref, gate_ref, up_ref, down_ref, out_ref):
-    sources = in_ref.shape[0]
-    rows = sources * SUB
+    groups = in_ref.shape[0]
+    rows = groups * SUB
     place = lax.broadcasted_iota(jnp.int32, (rows, LANE), 0) % SUB
-    kept = [in_ref[:, t].reshape(rows, LANE) for t in range(MAIN)]
-    tail = []
-    for q in range(TAIL):
-        spare = [
-            pltpu.roll(kept[3 * q + p].astype(jnp.float32), rows - SLOTS + 2 * p, 0)
-            for p in range(3)
+    units = gate_ref.shape[2]
+
+    def moved(x, places):
+        return pltpu.roll(x, places % rows, 0)
+
+    def by_place(first, second, third, spare):
+        rest = jnp.where(place < 4, second, jnp.where(place < SLOTS, third, spare))
+        return jnp.where(place < 2, first, rest)
+
+    came = [
+        [in_ref[:, i, t].reshape(rows, LANE).astype(jnp.float32) for t in range(MAIN)]
+        for i in range(4)
+    ]
+    x = []
+    for i in range(3):
+        blocks = [
+            jnp.where(place < SLOTS, came[i][t], moved(came[3][t], SLOTS - 2 * i))
+            for t in range(MAIN)
         ]
-        block = jnp.where(place < 2, spare[0], jnp.where(place < 4, spare[1], spare[2]))
-        tail.append(block.astype(jnp.bfloat16))
-    x = jnp.concatenate(kept + tail, axis=1)
+        for q in range(TAIL):
+            own = [moved(came[i][3 * q + p], 2 * p - SLOTS) for p in range(3)]
+            blocks.append(by_place(*own, came[3][3 * q + i]))
+        x.append(jnp.concatenate([block.astype(jnp.bfloat16) for block in blocks], axis=1))
+    x = jnp.concatenate(x, axis=0)
     hidden = []
-    units = gate_ref.shape[2]
     for lo in range(0, units, units // 2):
         half = slice(lo, lo + units // 2)
         gate_act = jnp.minimum(dot(x, gate_ref[0, :, half]), clamp_limit)
@@ -268,28 +281,38 @@
         hidden.append(act.astype(jnp.bfloat16))
     hidden = jnp.concatenate(hidden, axis=1)
     y_tail = dot(hidden, down_ref[0, :, MAIN * LANE :])
+
+    def part(y, i, c):
+        return y[i * rows : (i + 1) * rows, c * LANE : (c + 1) * LANE]
+
     for first in range(0, MAIN, TAIL):
         y = dot(hidden, down_ref[0, :, first * LANE : (first + TAIL) * LANE])
-        for i in range(TAIL):
-            t = first + i
+        for c in range(TAIL):
+            t = first + c
             q, p = t // 3, t % 3
-            spare = pltpu.roll(y_tail[:, q * LANE : (q + 1) * LANE], SLOTS - 2 * p, 0)
-            tile = jnp.where(place < SLOTS, y[:, i * LANE : (i + 1) * LANE], spare)
-            out_ref[:, t] = tile.astype(jnp.bfloat16).reshape(sources, SUB, LANE)
+            tiles = [
+                jnp.where(place < SLOTS, part(y, i, c), moved(part(y_tail, i, q), SLOTS - 2 * p))
+                for i in range(3)
+            ]
+            lent = [moved(part(y, i, c), 2 * i - SLOTS) for i in range(3)]
+            tiles.append(by_place(*lent, part(y_tail, p, q)))
+            for i, tile in enumerate(tiles):
+                out_ref[:, i, t] = tile.astype(jnp.bfloat16).reshape(groups, SUB, LANE)
 
 
 def expert(arrived, gate, up, down):
-    sources, step = arrived.shape[0], 64
-    block = pl.BlockSpec((step, MAIN, SUB, LANE), lambda i: (i, 0, 0, 0))
+    sources, step = arrived.shape[0], 32
+    fours = arrived.reshape(sources // 4, 4, *arrived.shape[1:])
+    block = pl.BlockSpec((step // 4, *fours.shape[1:]), lambda i: (i, 0, 0, 0, 0))
     whole = [pl.BlockSpec(w.shape, lambda i: (0, 0, 0)) for w in (gate, up, down)]
     return call(
         expert_body,
-        jax.ShapeDtypeStruct(arrived.shape, arrived.dtype),
-        36,
+        jax.ShapeDtypeStruct(fours.shape, fours.dtype),
+        30,
         grid=(sources // step,),
         in_specs=[block] + whole,
         out_specs=block,
-    )(arrived, gate, up, down)
+    )(fours, gate, up, down).reshape(arrived.shape)
 
 
 def combine_body(in_ref, blend_ref, first_ref, gain_ref, out_ref):

time: 156 us -> 155 us (level)
  no operation moved by 1% of the time
where the time goes in v4:
time: 155 us
  blocking collectives  138 us (89%)
  Pallas kernels  16.9 us (11%)
    all_to_all x4, blocking collectives, exchange(): return lax.all_to_all(x, axes, split_axis=0, concat_axis=0, tiled=True)  138 us
    pallas_call x1, Pallas kernels, expert(): call(expert_body, jax.ShapeDtypeStruct(fours.shape, fours.dtype), 30, gri...  6.76 us
    pallas_call x1, Pallas kernels, attend(): call(attend_body, (jax.ShapeDtypeStruct((parts, rows, size), qkv.dtype),...  3.45 us

profile of v4, /device:TPU:1, one launch (start us, length us, event | category | flops | bytes accessed | tf_op | source)
XLA Modules:
  0.0 154.8 jit_solution(9921513964515035)
XLA Ops:
  0.0 0.0 copy-start.5
  0.0 2.1 %shard_map.127 = (bf16[16,3,128,128]{3,2,1,0:T(8,128)(2,1)S(1)}, bf16[4,1024,128]{2,1,0:T(8,128)(2,1)S(1)}, bf16[4,128,1024]{2,1,0:T(8,128)(2,1)S(1)}) custom-call(bf16[1,128,2048]{2,1,0:T(8,128)(2,1)} %q_ref.1, bf16[1,128,2048]{2,1,0:T(8,128)(2,1)} %k_ref.1, bf16[1,128,2048]{2,1,0:T(8,128)(2,1)} %v_ref.1, s32[1,4,128]{2,1,0:T(4,128)} %bitcast.12, ...), custom_call_target="tpu_custom_call" | custom-call | tf_op jit(solution)/shard_map/pallas_call | solution.py:128
  2.1 30.0 %all_to_all.20.qkv_ref = bf16[16,3,128,128]{3,2,1,0:T(8,128)(2,1)S(1)} all-to-all(bf16[16,3,128,128]{3,2,1,0:T(8,128)(2,1)S(1)} %get-tuple-element.12), channel_id=1, replica_groups=mesh['sp_0'=4,'sp_1'=4,'dp'=8] {'sp_0','sp_1'}, dimensions={0} | all-to-all | bytes 3145728 | tf_op jit(solution)/shard_map/all_to_all | solution.py:344
  32.2 0.0 copy-done.5
  32.2 0.0 copy-start.3
  32.2 0.0 copy-start.6
  32.2 3.4 %shard_map.128 = (bf16[16,128,128]{2,1,0:T(8,128)(2,1)S(1)}, bf16[2048,2048]{1,0:T(8,128)(2,1)S(1)}) custom-call(bf16[16,3,128,128]{3,2,1,0:T(8,128)(2,1)S(1)} %all_to_all.20.qkv_ref, f32[1,2048]{1,0:T(1,128)S(1)} %bitcast.10, bf16[2048,2048]{1,0:T(8,128)(2,1)} %weight_ref.1), custom_call_target="tpu_custom_call" | custom-call | tf_op jit(solution)/shard_map/pallas_call | solution.py:199
  35.6 13.3 %all_to_all.21.heads_ref = bf16[16,128,128]{2,1,0:T(8,128)(2,1)S(1)} all-to-all(bf16[16,128,128]{2,1,0:T(8,128)(2,1)S(1)} %get-tuple-element.13), channel_id=1, replica_groups=mesh['sp_0'=4,'sp_1'=4,'dp'=8] {'sp_0','sp_1'}, dimensions={0} | all-to-all | bytes 1048576 | tf_op jit(solution)/shard_map/all_to_all | solution.py:344
  48.9 0.0 copy-done.3
  49.0 0.0 copy-done.6
  49.0 2.5 %shard_map.129 = (bf16[128,2048]{1,0:T(8,128)(2,1)S(1)}, bf16[128,12,8,128]{3,2,1,0:T(8,128)(2,1)S(1)}) custom-call(bf16[16,128,128]{2,1,0:T(8,128)(2,1)S(1)} %all_to_all.21.heads_ref, bf16[1,128,2048]{2,1,0:T(8,128)(2,1)S(1)} %copy-done.3, bf16[2048,2048]{1,0:T(8,128)(2,1)S(1)} %get-tuple-element.14.weight_ref, f32[1,2048]{1,0:T(1,128)S(1)} %bitcast.11, ...), custom_call_target="tpu_custom_call" | custom-call | tf_op jit(solution)/shard_map/pallas_call | solution.py:237
  51.5 0.0 copy-start
  51.5 0.0 copy-start.1
  51.5 0.0 copy-start.2
  51.5 48.8 %all_to_all.22 = bf16[128,12,8,128]{3,2,1,0:T(8,128)(2,1)S(1)} all-to-all(bf16[128,12,8,128]{3,2,1,0:T(8,128)(2,1)S(1)} %get-tuple-element.16), channel_id=1, replica_groups=mesh['sp_0'=4,'sp_1'=4,'dp'=8] {'sp_0','sp_1','dp'}, dimensions={0} | all-to-all | bytes 6291456 | tf_op jit(solution)/shard_map/all_to_all | solution.py:344
  100.3 0.0 copy-done
  100.3 0.0 copy-done.1
  100.3 0.0 copy-done.2
  100.3 6.8 %shard_map.130 = bf16[32,4,12,8,128]{4,3,2,1,0:T(8,128)(2,1)S(1)} custom-call(bf16[32,4,12,8,128]{4,3,2,1,0:T(8,128)(2,1)S(1)} %bitcast.7, bf16[1,2048,512]{2,1,0:T(8,128)(2,1)S(1)} %copy-done, bf16[1,2048,512]{2,1,0:T(8,128)(2,1)S(1)} %copy-done.1, bf16[1,512,2048]{2,1,0:T(8,128)(2,1)S(1)} %copy-done.2), custom_call_target="tpu_custom_call" | custom-call | tf_op jit(solution)/shard_map/pallas_call | solution.py:308
  107.1 0.0 copy-start.4
  107.1 45.6 %all_to_all.23.in_ref = bf16[128,12,8,128]{3,2,1,0:T(8,128)(2,1)S(1)} all-to-all(bf16[128,12,8,128]{3,2,1,0:T(8,128)(2,1)S(1)} %bitcast.8), channel_id=1, replica_groups=mesh['sp_0'=4,'sp_1'=4,'dp'=8] {'sp_0','sp_1','dp'}, dimensions={0} | all-to-all | bytes 6291456 | tf_op jit(solution)/shard_map/all_to_all | solution.py:344
  152.7 0.0 copy-done.4
  152.7 2.1 %shard_map.131 = bf16[1,128,2048]{2,1,0:T(8,128)(2,1)} custom-call(bf16[128,12,8,128]{3,2,1,0:T(8,128)(2,1)S(1)} %all_to_all.23.in_ref, bf16[4,128,1024]{2,1,0:T(8,128)(2,1)S(1)} %get-tuple-element.17.blend_ref, bf16[128,2048]{1,0:T(8,128)(2,1)S(1)} %get-tuple-element.18.first_ref, f32[1,2048]{1,0:T(1,128)S(1)} %bitcast.9), custom_call_target="tpu_custom_call" | custom-call | tf_op jit(solution)/shard_map/pallas_call | solution.py:336
Async XLA Ops:
  0.0 32.2 %copy-start.5 = (f32[1,1,2048]{2,1,0:T(1,128)S(1)}, f32[1,1,2048]{2,1,0:T(1,128)}, u32[]{:S(2)}) copy-start(f32[1,1,2048]{2,1,0:T(1,128)} %param.17) | copy-start | bytes 24580
  32.2 16.8 %copy-start.3 = (bf16[1,128,2048]{2,1,0:T(8,128)(2,1)S(1)}, bf16[1,128,2048]{2,1,0:T(8,128)(2,1)}, u32[]{:S(2)}) copy-start(bf16[1,128,2048]{2,1,0:T(8,128)(2,1)} %stream_ref.1) | copy-start | bytes 1572868
  32.2 16.8 %copy-start.6 = (f32[2048]{0:T(1024)S(1)}, f32[2048]{0:T(1024)}, u32[]{:S(2)}) copy-start(f32[2048]{0:T(1024)} %param.19) | copy-start | bytes 24580
  51.5 48.9 %copy-start = (bf16[1,2048,512]{2,1,0:T(8,128)(2,1)S(1)}, bf16[1,2048,512]{2,1,0:T(8,128)(2,1)}, u32[]{:S(2)}) copy-start(bf16[1,2048,512]{2,1,0:T(8,128)(2,1)} %gate_ref.1) | copy-start | bytes 6291460
  51.5 48.8 %copy-start.1 = (bf16[1,2048,512]{2,1,0:T(8,128)(2,1)S(1)}, bf16[1,2048,512]{2,1,0:T(8,128)(2,1)}, u32[]{:S(2)}) copy-start(bf16[1,2048,512]{2,1,0:T(8,128)(2,1)} %up_ref.1) | copy-start | bytes 6291460
  51.5 48.8 %copy-start.2 = (bf16[1,512,2048]{2,1,0:T(8,128)(2,1)S(1)}, bf16[1,512,2048]{2,1,0:T(8,128)(2,1)}, u32[]{:S(2)}) copy-start(bf16[1,512,2048]{2,1,0:T(8,128)(2,1)} %down_ref.1) | copy-start | bytes 6291460
  107.1 45.6 %copy-start.4 = (f32[2048]{0:T(1024)S(1)}, f32[2048]{0:T(1024)}, u32[]{:S(2)}) copy-start(f32[2048]{0:T(1024)} %param.25) | copy-start | bytes 24580

commit v5 on v4

v5 whole, which is shorter than its diff:
```python
import jax
import jax.numpy as jnp
from jax import lax
from jax.experimental import pallas as pl
from jax.experimental.pallas import tpu as pltpu
from jax.sharding import Mesh
from jax.sharding import PartitionSpec as P

SP = ("sp_0", "sp_1")
SP_DP = ("sp_0", "sp_1", "dp")

deep_alpha = 8.0**0.25
clamp_limit = 7.0
swish_alpha = 1.702
norm_eps = 1e-05
mask_fill = -1e30
log2_e = 1.4426950408889634

LANE = 128
SUB = 8
SLOTS = 6
MAIN = 12
TAIL = 4
MIB = 1 << 20


def call(body, out_shape, vmem_mib, **kwargs):
    return pl.pallas_call(
        body,
        out_shape=out_shape,
        compiler_params=pltpu.CompilerParams(vmem_limit_bytes=vmem_mib * MIB),
        **kwargs,
    )


def dot(a, b, dims=((1,), (0,))):
    return lax.dot_general(a, b, (dims, ((), ())), preferred_element_type=jnp.float32)


def layer_norm(summed, gain_row):
    centre = jnp.mean(summed, axis=-1, keepdims=True)
    centred = summed - centre
    spread = jnp.mean(jnp.square(centred), axis=-1, keepdims=True)
    return centred * lax.rsqrt(spread + norm_eps) * gain_row


def in_hbm(*arrays):
    return tuple(pltpu.with_memory_space_constraint(a, pltpu.HBM) for a in arrays)


def pack_body(q_ref, k_ref, v_ref, out_ref, land_ref, sems):
    copies = [
        pltpu.make_async_copy(ref.at[0], land_ref.at[n], sems.at[n])
        for n, ref in enumerate((q_ref, k_ref, v_ref))
    ]
    for copy in copies:
        copy.start()
    for n, copy in enumerate(copies):
        copy.wait()
        for h in range(out_ref.shape[0]):
            out_ref[h, n] = land_ref[n, :, h * LANE : (h + 1) * LANE]


def pack(q, k, v):
    rows, width = q.shape[1:]
    return call(
        pack_body,
        pltpu.VMEM((width // LANE, 3, rows, LANE), q.dtype),
        8,
        in_specs=[pl.BlockSpec(memory_space=pltpu.HBM)] * 3,
        out_specs=pl.BlockSpec(memory_space=pltpu.VMEM),
        scratch_shapes=[
            pltpu.VMEM((3, rows, width), q.dtype),
            pltpu.SemaphoreType.DMA((3,)),
        ],
    )(*in_hbm(q, k, v))


def attend_body(qkv_ref, gate_ref, weight_ref, out_ref, near_ref, score_ref, sem):
    brought = pltpu.make_async_copy(weight_ref, near_ref, sem)
    brought.start()
    parts, _, rows, size = qkv_ref.shape
    pair = 2
    block = pair * rows
    scale = size ** (-0.5) * log2_e

    def part(j, n):
        return qkv_ref[pair * j : pair * (j + 1), n].reshape(block, size)

    def score_rows(b):
        q = part(b, 0)
        base = gate_ref[:, block * b : block * b + 1]
        top = jnp.full((block, LANE), mask_fill, jnp.float32)
        for j in range(b + 1):
            bias = (gate_ref[:, block * j : block * (j + 1)] - base) * log2_e
            s = dot(q, part(j, 1), ((1,), (1,))) * scale - bias
            if j == b:
                row = lax.broadcasted_iota(jnp.int32, s.shape, 0)
                col = lax.broadcasted_iota(jnp.int32, s.shape, 1)
                s = jnp.where(row >= col, s, mask_fill)
            score_ref[b % 2, :, block * j : block * (j + 1)] = s
            for c in range(block // LANE):
                top = jnp.maximum(top, s[:, c * LANE : (c + 1) * LANE])
        return jnp.max(top, axis=1, keepdims=True)

    def blend_rows(b, row_max):
        total = jnp.zeros((block, LANE), jnp.float32)
        blended = jnp.zeros((block, size), jnp.float32)
        for j in range(b + 1):
            w = jnp.exp2(score_ref[b % 2, :, block * j : block * (j + 1)] - row_max)
            for c in range(block // LANE):
                total = total + w[:, c * LANE : (c + 1) * LANE]
            blended = blended + dot(w.astype(jnp.bfloat16), part(j, 2))
        row_total = jnp.sum(total, axis=1, keepdims=True)
        done = (blended / row_total).astype(jnp.bfloat16)
        out_ref[pair * b : pair * (b + 1)] = done.reshape(pair, rows, size)

    last = parts // pair - 1
    row_max = score_rows(last)
    for b in range(last, -1, -1):
        ahead = score_rows(b - 1) if b > 0 else None
        blend_rows(b, row_max)
        row_max = ahead
    brought.wait()


def attend(qkv, gates, weight):
    parts, _, rows, size = qkv.shape
    near = pl.BlockSpec(memory_space=pltpu.VMEM)
    return call(
        attend_body,
        (
            jax.ShapeDtypeStruct((parts, rows, size), qkv.dtype),
            pltpu.VMEM(weight.shape, weight.dtype),
        ),
        20,
        in_specs=[near, near, pl.BlockSpec(memory_space=pltpu.HBM)],
        out_specs=(near, near),
        scratch_shapes=[
            pltpu.VMEM((2, 2 * rows, parts * rows), jnp.float32),
            pltpu.SemaphoreType.DMA,
        ],
    )(qkv, gates, *in_hbm(weight))


def slot_of(place, kind):
    if kind == 0:
        return jnp.where(place < SLOTS, place, -2)
    return jnp.where(place >= SLOTS, place - SLOTS + 2 * (kind - 1), -2)


def route_into(ids_ref, score_ref, pick_ref, blend_ref):
    top_k, rows = ids_ref.shape[1:]
    experts = pick_ref.shape[1] // SUB
    expert = lax.broadcasted_iota(jnp.int32, (experts, rows), 0)
    scores = score_ref[0]
    raised = jnp.exp(scores - jnp.max(scores, axis=0, keepdims=True))
    shares = raised / jnp.sum(raised, axis=0, keepdims=True)
    named = jnp.zeros((experts, rows), jnp.float32)
    share = jnp.zeros((experts, rows), jnp.float32)
    for k in range(top_k):
        hit = ids_ref[0, k : k + 1] == expert
        named = jnp.where(hit, 1.0, named)
        share = jnp.where(hit, shares[k : k + 1], share)
    earlier = lax.broadcasted_iota(jnp.int32, (rows, rows), 0) < lax.broadcasted_iota(
        jnp.int32, (rows, rows), 1
    )
    rank = dot(named.astype(jnp.bfloat16), jnp.where(earlier, 1.0, 0.0).astype(jnp.bfloat16))
    slot = jnp.where(named > 0.0, rank, -1.0)
    by_expert = jnp.broadcast_to(slot[:, None, :], (experts, SUB, rows))
    place = lax.broadcasted_iota(jnp.int32, (experts, SUB, rows), 1)
    for kind in range(4):
        hit = by_expert == slot_of(place, kind).astype(jnp.float32)
        pick = jnp.where(hit, 1.0, 0.0).reshape(experts * SUB, rows).astype(jnp.bfloat16)
        pick_ref[kind] = pick
    wide = (experts, experts * SUB)
    spread = lax.broadcasted_iota(jnp.int32, wide, 0) == lax.broadcasted_iota(
        jnp.int32, wide, 1
    ) // SUB
    spread = jnp.where(spread, 1.0, 0.0).astype(jnp.bfloat16)
    wide_slot = dot(slot.T.astype(jnp.bfloat16), spread)
    wide_share = dot(share.T.astype(jnp.bfloat16), spread)
    place = lax.broadcasted_iota(jnp.int32, wide_slot.shape, 1) % SUB
    for kind in range(4):
        hit = wide_slot == slot_of(place, kind).astype(jnp.float32)
        blend_ref[kind] = jnp.where(hit, wide_share, 0.0).astype(jnp.bfloat16)


def project_body(
    heads_ref,
    stream_ref,
    weight_ref,
    gain_ref,
    ids_ref,
    score_ref,
    first_ref,
    out_ref,
    blend_ref,
    pick_ref,
):
    heads = heads_ref.shape[0]
    experts = out_ref.shape[0]
    attended = jnp.concatenate([heads_ref[h] for h in range(heads)], axis=1)
    projected = dot(attended, weight_ref[...])
    route_into(ids_ref, score_ref, pick_ref, blend_ref)
    summed = deep_alpha * stream_ref[0].astype(jnp.float32) + projected
    first = layer_norm(summed, gain_ref[...]).astype(jnp.bfloat16)
    first_ref[...] = first
    tail = first[:, MAIN * LANE :]
    for p in range(3):
        kept = [first[:, (3 * q + p) * LANE : (3 * q + p + 1) * LANE] for q in range(TAIL)]
        both = jnp.concatenate([jnp.concatenate(kept, axis=1), tail], axis=0)
        lhs = jnp.concatenate([pick_ref[0], pick_ref[p + 1]], axis=1)
        rows = dot(lhs, both).astype(jnp.bfloat16)
        for q in range(TAIL):
            tile = rows[:, q * LANE : (q + 1) * LANE]
            out_ref[:, 3 * q + p] = tile.reshape(experts, SUB, LANE)


def project(heads, stream, weight, gain, ids, scores, experts):
    rows, width = stream.shape[1:]
    return call(
        project_body,
        (
            jax.ShapeDtypeStruct((rows, width), jnp.bfloat16),
            jax.ShapeDtypeStruct((experts, MAIN, SUB, LANE), jnp.bfloat16),
            jax.ShapeDtypeStruct((4, rows, experts * SUB), jnp.bfloat16),
        ),
        36,
        scratch_shapes=[pltpu.VMEM((4, experts * SUB, rows), jnp.bfloat16)],
    )(heads, stream, weight, gain, ids, scores)


def expert_body(in_ref, gate_ref, up_ref, down_ref, out_ref):
    groups = in_ref.shape[0]
    rows = groups * SUB
    units = gate_ref.shape[2]
    place = lax.broadcasted_iota(jnp.int32, (rows, LANE), 0) % SUB
    place = place.astype(jnp.int16)
    below = [place < jnp.int16(n) for n in (2, 4, SLOTS)]

    def moved(x, places):
        return pltpu.roll(x, places % rows, 0)

    def by_place(first, second, third, spare):
        rest = jnp.where(below[1], second, jnp.where(below[2], third, spare))
        return jnp.where(below[0], first, rest)

    came = [[in_ref[:, i, t].reshape(rows, LANE) for t in range(MAIN)] for i in range(4)]
    x = []
    for i in range(3):
        blocks = [
            jnp.where(below[2], came[i][t], moved(came[3][t], SLOTS - 2 * i)) for t in range(MAIN)
        ]
        for q in range(TAIL):
            own = [moved(came[i][3 * q + p], 2 * p - SLOTS) for p in range(3)]
            blocks.append(by_place(*own, came[3][3 * q + i]))
        x.append(jnp.concatenate(blocks, axis=1))
    x = jnp.concatenate(x, axis=0)
    hidden = []
    for lo in range(0, units, units // 2):
        half = slice(lo, lo + units // 2)
        gate_act = jnp.minimum(dot(x, gate_ref[0, :, half]), clamp_limit)
        up_act = jnp.clip(dot(x, up_ref[0, :, half]), -clamp_limit, clamp_limit)
        act = gate_act * jax.nn.sigmoid(swish_alpha * gate_act) * (up_act + 1.0)
        hidden.append(act.astype(jnp.bfloat16))
    hidden = jnp.concatenate(hidden, axis=1)
    y_tail = dot(hidden, down_ref[0, :, MAIN * LANE :]).astype(jnp.bfloat16)

    def part(y, i, c):
        return y[i * rows : (i + 1) * rows, c * LANE : (c + 1) * LANE]

    for first in range(0, MAIN, TAIL):
        y = dot(hidden, down_ref[0, :, first * LANE : (first + TAIL) * LANE])
        y = y.astype(jnp.bfloat16)
        for c in range(TAIL):
            t = first + c
            q, p = t // 3, t % 3
            tiles = [
                jnp.where(below[2], part(y, i, c), moved(part(y_tail, i, q), SLOTS - 2 * p))
                for i in range(3)
            ]
            lent = [moved(part(y, i, c), 2 * i - SLOTS) for i in range(3)]
            tiles.append(by_place(*lent, part(y_tail, p, q)))
            for i, tile in enumerate(tiles):
                out_ref[:, i, t] = tile.reshape(groups, SUB, LANE)


def expert(arrived, gate, up, down):
    sources, step = arrived.shape[0], 64
    fours = arrived.reshape(sources // 4, 4, *arrived.shape[1:])
    block = pl.BlockSpec((step // 4, *fours.shape[1:]), lambda i: (i, 0, 0, 0, 0))
    whole = [pl.BlockSpec(w.shape, lambda i: (0, 0, 0)) for w in (gate, up, down)]
    return call(
        expert_body,
        jax.ShapeDtypeStruct(fours.shape, fours.dtype),
        30,
        grid=(sources // step,),
        in_specs=[block] + whole,
        out_specs=block,
    )(fours, gate, up, down).reshape(arrived.shape)


def combine_body(in_ref, blend_ref, first_ref, gain_ref, out_ref):
    experts = in_ref.shape[0]
    tail = None
    blocks = [None] * MAIN
    for p in range(3):
        rows = [in_ref[:, 3 * q + p].reshape(experts * SUB, LANE) for q in range(TAIL)]
        both = jnp.concatenate([blend_ref[0], blend_ref[p + 1]], axis=0)
        mixed = dot(both, jnp.concatenate(rows, axis=1))
        count = blend_ref.shape[1]
        for q in range(TAIL):
            blocks[3 * q + p] = mixed[:count, q * LANE : (q + 1) * LANE]
        tail = mixed[count:] if tail is None else tail + mixed[count:]
    mixture = jnp.concatenate(blocks + [tail], axis=1)
    summed = deep_alpha * first_ref[...].astype(jnp.float32) + mixture
    out_ref[0] = layer_norm(summed, gain_ref[...]).astype(jnp.bfloat16)


def combine(returned, blend, first, gain):
    return call(
        combine_body,
        jax.ShapeDtypeStruct((1, *first.shape), jnp.bfloat16),
        36,
    )(returned, blend, first, gain)


def exchange(x, axes):
    return lax.all_to_all(x, axes, split_axis=0, concat_axis=0, tiled=True)


def shards(
    stream,
    query_rows,
    key_rows,
    value_rows,
    forget_sums,
    out_weight,
    first_gain,
    expert_ids,
    route_scores,
    gate_weight,
    up_weight,
    down_weight,
    second_gain,
):
    experts = lax.axis_size(SP_DP)
    qkv = exchange(pack(query_rows, key_rows, value_rows), SP)
    attended, near_weight = attend(qkv, forget_sums[0], out_weight)
    heads = exchange(attended, SP)
    first, outgoing, blend = project(
        heads,
        stream,
        near_weight,
        first_gain[None],
        expert_ids.transpose(0, 2, 1),
        route_scores.transpose(0, 2, 1),
        experts,
    )
    arrived = exchange(outgoing, SP_DP)
    finished = expert(arrived, gate_weight, up_weight, down_weight)
    returned = exchange(finished, SP_DP)
    return combine(returned, blend, first, second_gain[None])


def solution(mesh):
    finer = Mesh(mesh.devices.reshape(4, 4, mesh.shape["dp"]), ("sp_0", "sp_1", "dp"))
    rows = P("dp", SP, None)
    own = P(SP_DP, None, None)
    placed = (rows,) * 5 + (P(), P(), rows, rows, own, own, own, P())
    return jax.shard_map(shards, mesh=finer, in_specs=placed, out_specs=rows, check_vma=False)
```

time: 155 us -> 154 us (level)
  no operation moved by 1% of the time
where the time goes in v5:
time: 154 us; the launch traced here: 153 us
  blocking collectives  138 us (90%)
  Pallas kernels  15.4 us (10%)
    all_to_all x4, blocking collectives, exchange(): return lax.all_to_all(x, axes, split_axis=0, concat_axis=0, tiled=True)  138 us
    pallas_call x1, Pallas kernels, expert(): call(expert_body, jax.ShapeDtypeStruct(fours.shape, fours.dtype), 30, gri...  5.51 us
    pallas_call x1, Pallas kernels, attend(): call(attend_body, (jax.ShapeDtypeStruct((parts, rows, size), qkv.dtype),...  3.45 us

profile of v5, /device:TPU:1, one launch (start us, length us, event | category | flops | bytes accessed | tf_op | source)
XLA Modules:
  0.0 153.3 jit_solution(12443143874390561981)
XLA Ops:
  0.0 0.0 copy-start.6
  0.0 1.5 shard_map.127
  1.5 30.0 %all_to_all.20.qkv_ref = bf16[16,3,128,128]{3,2,1,0:T(8,128)(2,1)S(1)} all-to-all(bf16[16,3,128,128]{3,2,1,0:T(8,128)(2,1)S(1)} %shard_map.127), channel_id=1, replica_groups=mesh['sp_0'=4,'sp_1'=4,'dp'=8] {'sp_0','sp_1'}, dimensions={0} | all-to-all | bytes 3145728 | tf_op jit(solution)/shard_map/all_to_all | solution.py:330
  31.5 0.0 copy-done.6
  31.5 0.0 copy-start.3
  31.5 0.0 copy-start.4
  31.6 0.0 copy-start.7
  31.6 0.0 copy-start.8
  31.6 3.4 %shard_map.128 = (bf16[16,128,128]{2,1,0:T(8,128)(2,1)S(1)}, bf16[2048,2048]{1,0:T(8,128)(2,1)S(1)}) custom-call(bf16[16,3,128,128]{3,2,1,0:T(8,128)(2,1)S(1)} %all_to_all.20.qkv_ref, f32[1,2048]{1,0:T(1,128)S(1)} %bitcast.11, bf16[2048,2048]{1,0:T(8,128)(2,1)} %weight_ref.1), custom_call_target="tpu_custom_call" | custom-call | tf_op jit(solution)/shard_map/pallas_call | solution.py:130
  35.0 13.3 %all_to_all.21.heads_ref = bf16[16,128,128]{2,1,0:T(8,128)(2,1)S(1)} all-to-all(bf16[16,128,128]{2,1,0:T(8,128)(2,1)S(1)} %get-tuple-element.10), channel_id=1, replica_groups=mesh['sp_0'=4,'sp_1'=4,'dp'=8] {'sp_0','sp_1'}, dimensions={0} | all-to-all | bytes 1048576 | tf_op jit(solution)/shard_map/all_to_all | solution.py:330
  48.3 0.0 copy-done.3
  48.4 0.0 copy-done.4
  48.4 0.0 copy-done.7
  48.4 0.0 copy-done.8
  48.4 2.8 %shard_map.129 = (bf16[128,2048]{1,0:T(8,128)(2,1)S(1)}, bf16[128,12,8,128]{3,2,1,0:T(8,128)(2,1)S(1)}, bf16[4,128,1024]{2,1,0:T(8,128)(2,1)S(1)}) custom-call(bf16[16,128,128]{2,1,0:T(8,128)(2,1)S(1)} %all_to_all.21.heads_ref, bf16[1,128,2048]{2,1,0:T(8,128)(2,1)S(1)} %copy-done.3, bf16[2048,2048]{1,0:T(8,128)(2,1)S(1)} %get-tuple-element.11.weight_ref, ...), custom_call_target="tpu_custom_call" | custom-call | tf_op jit(solution)/shard_map/pallas_call | solution.py:222
  51.2 0.0 copy-start
  51.2 0.0 copy-start.1
  51.2 0.0 copy-start.2
  51.3 48.8 %all_to_all.22 = bf16[128,12,8,128]{3,2,1,0:T(8,128)(2,1)S(1)} all-to-all(bf16[128,12,8,128]{3,2,1,0:T(8,128)(2,1)S(1)} %get-tuple-element.12), channel_id=1, replica_groups=mesh['sp_0'=4,'sp_1'=4,'dp'=8] {'sp_0','sp_1','dp'}, dimensions={0} | all-to-all | bytes 6291456 | tf_op jit(solution)/shard_map/all_to_all | solution.py:330
  100.1 0.0 copy-done
  100.1 0.0 copy-done.1
  100.1 0.0 copy-done.2
  100.1 5.5 %shard_map.130 = bf16[32,4,12,8,128]{4,3,2,1,0:T(8,128)(2,1)S(1)} custom-call(bf16[32,4,12,8,128]{4,3,2,1,0:T(8,128)(2,1)S(1)} %bitcast.7, bf16[1,2048,512]{2,1,0:T(8,128)(2,1)S(1)} %copy-done, bf16[1,2048,512]{2,1,0:T(8,128)(2,1)S(1)} %copy-done.1, bf16[1,512,2048]{2,1,0:T(8,128)(2,1)S(1)} %copy-done.2), custom_call_target="tpu_custom_call" | custom-call | tf_op jit(solution)/shard_map/pallas_call | solution.py:294
  105.6 0.0 copy-start.5
  105.6 45.6 %all_to_all.23.in_ref = bf16[128,12,8,128]{3,2,1,0:T(8,128)(2,1)S(1)} all-to-all(bf16[128,12,8,128]{3,2,1,0:T(8,128)(2,1)S(1)} %bitcast.8), channel_id=1, replica_groups=mesh['sp_0'=4,'sp_1'=4,'dp'=8] {'sp_0','sp_1','dp'}, dimensions={0} | all-to-all | bytes 6291456 | tf_op jit(solution)/shard_map/all_to_all | solution.py:330
  151.2 0.0 copy-done.5
  151.2 2.1 %shard_map.131 = bf16[1,128,2048]{2,1,0:T(8,128)(2,1)} custom-call(bf16[128,12,8,128]{3,2,1,0:T(8,128)(2,1)S(1)} %all_to_all.23.in_ref, bf16[4,128,1024]{2,1,0:T(8,128)(2,1)S(1)} %get-tuple-element.13.blend_ref, bf16[128,2048]{1,0:T(8,128)(2,1)S(1)} %get-tuple-element.14.first_ref, f32[1,2048]{1,0:T(1,128)S(1)} %bitcast.10), custom_call_target="tpu_custom_call" | custom-call | tf_op jit(solution)/shard_map/pallas_call | solution.py:322
Async XLA Ops:
  0.0 31.5 %copy-start.6 = (f32[1,1,2048]{2,1,0:T(1,128)S(1)}, f32[1,1,2048]{2,1,0:T(1,128)}, u32[]{:S(2)}) copy-start(f32[1,1,2048]{2,1,0:T(1,128)} %param.17) | copy-start | bytes 24580
  31.5 16.8 %copy-start.3 = (bf16[1,128,2048]{2,1,0:T(8,128)(2,1)S(1)}, bf16[1,128,2048]{2,1,0:T(8,128)(2,1)}, u32[]{:S(2)}) copy-start(bf16[1,128,2048]{2,1,0:T(8,128)(2,1)} %stream_ref.1) | copy-start | bytes 1572868
  31.5 16.8 %copy-start.4 = (f32[2048]{0:T(1024)S(1)}, f32[2048]{0:T(1024)}, u32[]{:S(2)}) copy-start(f32[2048]{0:T(1024)} %param.19) | copy-start | bytes 24580
  31.6 16.8 %copy-start.7 = (s32[1,128,4]{1,2,0:T(4,128)S(1)}, s32[1,128,4]{1,2,0:T(4,128)}, u32[]{:S(2)}) copy-start(s32[1,128,4]{1,2,0:T(4,128)} %param.20) | copy-start | bytes 6148
  31.6 16.8 %copy-start.8 = (f32[1,128,4]{1,2,0:T(4,128)S(1)}, f32[1,128,4]{1,2,0:T(4,128)}, u32[]{:S(2)}) copy-start(f32[1,128,4]{1,2,0:T(4,128)} %param.21) | copy-start | bytes 6148
  51.2 48.9 %copy-start = (bf16[1,2048,512]{2,1,0:T(8,128)(2,1)S(1)}, bf16[1,2048,512]{2,1,0:T(8,128)(2,1)}, u32[]{:S(2)}) copy-start(bf16[1,2048,512]{2,1,0:T(8,128)(2,1)} %gate_ref.1) | copy-start | bytes 6291460
  51.2 48.9 %copy-start.1 = (bf16[1,2048,512]{2,1,0:T(8,128)(2,1)S(1)}, bf16[1,2048,512]{2,1,0:T(8,128)(2,1)}, u32[]{:S(2)}) copy-start(bf16[1,2048,512]{2,1,0:T(8,128)(2,1)} %up_ref.1) | copy-start | bytes 6291460
  51.2 48.8 %copy-start.2 = (bf16[1,512,2048]{2,1,0:T(8,128)(2,1)S(1)}, bf16[1,512,2048]{2,1,0:T(8,128)(2,1)}, u32[]{:S(2)}) copy-start(bf16[1,512,2048]{2,1,0:T(8,128)(2,1)} %down_ref.1) | copy-start | bytes 6291460
  105.6 45.6 %copy-start.5 = (f32[2048]{0:T(1024)S(1)}, f32[2048]{0:T(1024)}, u32[]{:S(2)}) copy-start(f32[2048]{0:T(1024)} %param.25) | copy-start | bytes 24580

commit v6 on v5

--- a/solution.py
+++ b/solution.py
@@ -1,3 +1,5 @@
+import functools
+
 import jax
 import jax.numpy as jnp
 from jax import lax
@@ -8,6 +10,7 @@
 
 SP = ("sp_0", "sp_1")
 SP_DP = ("sp_0", "sp_1", "dp")
+DP_SP = ("dp", "sp_0", "sp_1")
 
 deep_alpha = 8.0**0.25
 clamp_limit = 7.0
@@ -149,10 +152,12 @@
     return jnp.where(place >= SLOTS, place - SLOTS + 2 * (kind - 1), -2)
 
 
-def route_into(ids_ref, score_ref, pick_ref, blend_ref):
+def route_into(ids_ref, score_ref, pick_ref, blend_ref, dp_count):
     top_k, rows = ids_ref.shape[1:]
     experts = pick_ref.shape[1] // SUB
-    expert = lax.broadcasted_iota(jnp.int32, (experts, rows), 0)
+    turn = lax.broadcasted_iota(jnp.int32, (experts, rows), 0)
+    sp_count = experts // dp_count
+    expert = turn % sp_count * dp_count + turn // sp_count
     scores = score_ref[0]
     raised = jnp.exp(scores - jnp.max(scores, axis=0, keepdims=True))
     shares = raised / jnp.sum(raised, axis=0, keepdims=True)
@@ -197,12 +202,14 @@
     out_ref,
     blend_ref,
     pick_ref,
+    *,
+    dp_count,
 ):
     heads = heads_ref.shape[0]
     experts = out_ref.shape[0]
     attended = jnp.concatenate([heads_ref[h] for h in range(heads)], axis=1)
     projected = dot(attended, weight_ref[...])
-    route_into(ids_ref, score_ref, pick_ref, blend_ref)
+    route_into(ids_ref, score_ref, pick_ref, blend_ref, dp_count)
     summed = deep_alpha * stream_ref[0].astype(jnp.float32) + projected
     first = layer_norm(summed, gain_ref[...]).astype(jnp.bfloat16)
     first_ref[...] = first
@@ -217,10 +224,10 @@
             out_ref[:, 3 * q + p] = tile.reshape(experts, SUB, LANE)
 
 
-def project(heads, stream, weight, gain, ids, scores, experts):
+def project(heads, stream, weight, gain, ids, scores, experts, dp_count):
     rows, width = stream.shape[1:]
     return call(
-        project_body,
+        functools.partial(project_body, dp_count=dp_count),
         (
             jax.ShapeDtypeStruct((rows, width), jnp.bfloat16),
             jax.ShapeDtypeStruct((experts, MAIN, SUB, LANE), jnp.bfloat16),
@@ -357,10 +364,11 @@
         expert_ids.transpose(0, 2, 1),
         route_scores.transpose(0, 2, 1),
         experts,
+        lax.axis_size("dp"),
     )
-    arrived = exchange(outgoing, SP_DP)
+    arrived = exchange(outgoing, DP_SP)
     finished = expert(arrived, gate_weight, up_weight, down_weight)
-    returned = exchange(finished, SP_DP)
+    returned = exchange(finished, DP_SP)
     return combine(returned, blend, first, second_gain[None])
 
 

time: 154 us -> 152 us (0.987)
  blocking collectives: 138 us -> 136 us
where the time goes in v6:
time: 152 us
  blocking collectives  136 us (89%)
  Pallas kernels  15.4 us (10%)
    all_to_all x4, blocking collectives, exchange(): return lax.all_to_all(x, axes, split_axis=0, concat_axis=0, tiled=True)  136 us
    pallas_call x1, Pallas kernels, expert(): call(expert_body, jax.ShapeDtypeStruct(fours.shape, fours.dtype), 30, gri...  5.51 us
    pallas_call x1, Pallas kernels, attend(): call(attend_body, (jax.ShapeDtypeStruct((parts, rows, size), qkv.dtype),...  3.45 us

profile of v6, /device:TPU:1, one launch (start us, length us, event | category | flops | bytes accessed | tf_op | source)
XLA Modules:
  0.0 151.8 jit_solution(15260568361035006891)
XLA Ops:
  0.0 0.0 copy-start.6
  0.0 1.5 shard_map.127
  1.5 30.0 %all_to_all.20.qkv_ref = bf16[16,3,128,128]{3,2,1,0:T(8,128)(2,1)S(1)} all-to-all(bf16[16,3,128,128]{3,2,1,0:T(8,128)(2,1)S(1)} %shard_map.127), channel_id=1, replica_groups=mesh['sp_0'=4,'sp_1'=4,'dp'=8] {'sp_0','sp_1'}, dimensions={0} | all-to-all | bytes 3145728 | tf_op jit(solution)/shard_map/all_to_all | solution.py:337
  31.5 0.0 copy-done.6
  31.5 0.0 copy-start.3
  31.5 0.0 copy-start.4
  31.6 0.0 copy-start.7
  31.6 0.0 copy-start.8
  31.6 3.4 %shard_map.128 = (bf16[16,128,128]{2,1,0:T(8,128)(2,1)S(1)}, bf16[2048,2048]{1,0:T(8,128)(2,1)S(1)}) custom-call(bf16[16,3,128,128]{3,2,1,0:T(8,128)(2,1)S(1)} %all_to_all.20.qkv_ref, f32[1,2048]{1,0:T(1,128)S(1)} %bitcast.11, bf16[2048,2048]{1,0:T(8,128)(2,1)} %weight_ref.1), custom_call_target="tpu_custom_call" | custom-call | tf_op jit(solution)/shard_map/pallas_call | solution.py:133
  35.0 13.3 %all_to_all.21.heads_ref = bf16[16,128,128]{2,1,0:T(8,128)(2,1)S(1)} all-to-all(bf16[16,128,128]{2,1,0:T(8,128)(2,1)S(1)} %get-tuple-element.10), channel_id=1, replica_groups=mesh['sp_0'=4,'sp_1'=4,'dp'=8] {'sp_0','sp_1'}, dimensions={0} | all-to-all | bytes 1048576 | tf_op jit(solution)/shard_map/all_to_all | solution.py:337
  48.3 0.0 copy-done.3
  48.4 0.0 copy-done.4
  48.4 0.0 copy-done.7
  48.4 0.0 copy-done.8
  48.4 2.8 %shard_map.129 = (bf16[128,2048]{1,0:T(8,128)(2,1)S(1)}, bf16[128,12,8,128]{3,2,1,0:T(8,128)(2,1)S(1)}, bf16[4,128,1024]{2,1,0:T(8,128)(2,1)S(1)}) custom-call(bf16[16,128,128]{2,1,0:T(8,128)(2,1)S(1)} %all_to_all.21.heads_ref, bf16[1,128,2048]{2,1,0:T(8,128)(2,1)S(1)} %copy-done.3, bf16[2048,2048]{1,0:T(8,128)(2,1)S(1)} %get-tuple-element.11.weight_ref, ...), custom_call_target="tpu_custom_call" | custom-call | tf_op jit(solution)/shard_map/pallas_call | solution.py:229
  51.2 0.0 copy-start
  51.2 0.0 copy-start.1
  51.2 0.0 copy-start.2
  51.2 47.6 %all_to_all.22 = bf16[128,12,8,128]{3,2,1,0:T(8,128)(2,1)S(1)} all-to-all(bf16[128,12,8,128]{3,2,1,0:T(8,128)(2,1)S(1)} %get-tuple-element.12), channel_id=1, replica_groups=mesh['sp_0'=4,'sp_1'=4,'dp'=8] {'dp','sp_0','sp_1'}, dimensions={0} | all-to-all | bytes 6291456 | tf_op jit(solution)/shard_map/all_to_all | solution.py:337
  98.8 0.0 copy-done
  98.8 0.0 copy-done.1
  98.8 0.0 copy-done.2
  98.8 5.5 %shard_map.130 = bf16[32,4,12,8,128]{4,3,2,1,0:T(8,128)(2,1)S(1)} custom-call(bf16[32,4,12,8,128]{4,3,2,1,0:T(8,128)(2,1)S(1)} %bitcast.7, bf16[1,2048,512]{2,1,0:T(8,128)(2,1)S(1)} %copy-done, bf16[1,2048,512]{2,1,0:T(8,128)(2,1)S(1)} %copy-done.1, bf16[1,512,2048]{2,1,0:T(8,128)(2,1)S(1)} %copy-done.2), custom_call_target="tpu_custom_call" | custom-call | tf_op jit(solution)/shard_map/pallas_call | solution.py:301
  104.3 0.0 copy-start.5
  104.3 45.4 %all_to_all.23.in_ref = bf16[128,12,8,128]{3,2,1,0:T(8,128)(2,1)S(1)} all-to-all(bf16[128,12,8,128]{3,2,1,0:T(8,128)(2,1)S(1)} %bitcast.8), channel_id=1, replica_groups=mesh['sp_0'=4,'sp_1'=4,'dp'=8] {'dp','sp_0','sp_1'}, dimensions={0} | all-to-all | bytes 6291456 | tf_op jit(solution)/shard_map/all_to_all | solution.py:337
  149.7 0.0 copy-done.5
  149.7 2.1 %shard_map.131 = bf16[1,128,2048]{2,1,0:T(8,128)(2,1)} custom-call(bf16[128,12,8,128]{3,2,1,0:T(8,128)(2,1)S(1)} %all_to_all.23.in_ref, bf16[4,128,1024]{2,1,0:T(8,128)(2,1)S(1)} %get-tuple-element.13.blend_ref, bf16[128,2048]{1,0:T(8,128)(2,1)S(1)} %get-tuple-element.14.first_ref, f32[1,2048]{1,0:T(1,128)S(1)} %bitcast.10), custom_call_target="tpu_custom_call" | custom-call | tf_op jit(solution)/shard_map/pallas_call | solution.py:329
Async XLA Ops:
  0.0 31.5 %copy-start.6 = (f32[1,1,2048]{2,1,0:T(1,128)S(1)}, f32[1,1,2048]{2,1,0:T(1,128)}, u32[]{:S(2)}) copy-start(f32[1,1,2048]{2,1,0:T(1,128)} %param.17) | copy-start | bytes 24580
  31.5 16.8 %copy-start.3 = (bf16[1,128,2048]{2,1,0:T(8,128)(2,1)S(1)}, bf16[1,128,2048]{2,1,0:T(8,128)(2,1)}, u32[]{:S(2)}) copy-start(bf16[1,128,2048]{2,1,0:T(8,128)(2,1)} %stream_ref.1) | copy-start | bytes 1572868
  31.5 16.8 %copy-start.4 = (f32[2048]{0:T(1024)S(1)}, f32[2048]{0:T(1024)}, u32[]{:S(2)}) copy-start(f32[2048]{0:T(1024)} %param.19) | copy-start | bytes 24580
  31.6 16.8 %copy-start.7 = (s32[1,128,4]{1,2,0:T(4,128)S(1)}, s32[1,128,4]{1,2,0:T(4,128)}, u32[]{:S(2)}) copy-start(s32[1,128,4]{1,2,0:T(4,128)} %param.20) | copy-start | bytes 6148
  31.6 16.8 %copy-start.8 = (f32[1,128,4]{1,2,0:T(4,128)S(1)}, f32[1,128,4]{1,2,0:T(4,128)}, u32[]{:S(2)}) copy-start(f32[1,128,4]{1,2,0:T(4,128)} %param.21) | copy-start | bytes 6148
  51.2 47.6 %copy-start = (bf16[1,2048,512]{2,1,0:T(8,128)(2,1)S(1)}, bf16[1,2048,512]{2,1,0:T(8,128)(2,1)}, u32[]{:S(2)}) copy-start(bf16[1,2048,512]{2,1,0:T(8,128)(2,1)} %gate_ref.1) | copy-start | bytes 6291460
  51.2 47.6 %copy-start.1 = (bf16[1,2048,512]{2,1,0:T(8,128)(2,1)S(1)}, bf16[1,2048,512]{2,1,0:T(8,128)(2,1)}, u32[]{:S(2)}) copy-start(bf16[1,2048,512]{2,1,0:T(8,128)(2,1)} %up_ref.1) | copy-start | bytes 6291460
  51.2 47.6 %copy-start.2 = (bf16[1,512,2048]{2,1,0:T(8,128)(2,1)S(1)}, bf16[1,512,2048]{2,1,0:T(8,128)(2,1)}, u32[]{:S(2)}) copy-start(bf16[1,512,2048]{2,1,0:T(8,128)(2,1)} %down_ref.1) | copy-start | bytes 6291460
  104.3 45.4 %copy-start.5 = (f32[2048]{0:T(1024)S(1)}, f32[2048]{0:T(1024)}, u32[]{:S(2)}) copy-start(f32[2048]{0:T(1024)} %param.25) | copy-start | bytes 24580

commit v7 on v6

--- a/solution.py
+++ b/solution.py
@@ -9,8 +9,9 @@
 from jax.sharding import PartitionSpec as P
 
 SP = ("sp_0", "sp_1")
-SP_DP = ("sp_0", "sp_1", "dp")
-DP_SP = ("dp", "sp_0", "sp_1")
+DP = ("x_1", "x_0", "core")
+SP_DP = SP + DP
+DP_SP = ("x_0", "x_1", "core") + SP
 
 deep_alpha = 8.0**0.25
 clamp_limit = 7.0
@@ -157,7 +158,10 @@
     experts = pick_ref.shape[1] // SUB
     turn = lax.broadcasted_iota(jnp.int32, (experts, rows), 0)
     sp_count = experts // dp_count
-    expert = turn % sp_count * dp_count + turn // sp_count
+    outer = turn // sp_count
+    quarter = dp_count // 4
+    x_0, x_1 = outer // (2 * quarter), outer // quarter % 2
+    expert = turn % sp_count * dp_count + (2 * x_1 + x_0) * quarter + outer % quarter
     scores = score_ref[0]
     raised = jnp.exp(scores - jnp.max(scores, axis=0, keepdims=True))
     shares = raised / jnp.sum(raised, axis=0, keepdims=True)
@@ -277,10 +281,11 @@
     def part(y, i, c):
         return y[i * rows : (i + 1) * rows, c * LANE : (c + 1) * LANE]
 
-    for first in range(0, MAIN, TAIL):
-        y = dot(hidden, down_ref[0, :, first * LANE : (first + TAIL) * LANE])
+    step = MAIN // 2
+    for first in range(0, MAIN, step):
+        y = dot(hidden, down_ref[0, :, first * LANE : (first + step) * LANE])
         y = y.astype(jnp.bfloat16)
-        for c in range(TAIL):
+        for c in range(step):
             t = first + c
             q, p = t // 3, t % 3
             tiles = [
@@ -364,7 +369,7 @@
         expert_ids.transpose(0, 2, 1),
         route_scores.transpose(0, 2, 1),
         experts,
-        lax.axis_size("dp"),
+        lax.axis_size(DP),
     )
     arrived = exchange(outgoing, DP_SP)
     finished = expert(arrived, gate_weight, up_weight, down_weight)
@@ -373,8 +378,8 @@
 
 
 def solution(mesh):
-    finer = Mesh(mesh.devices.reshape(4, 4, mesh.shape["dp"]), ("sp_0", "sp_1", "dp"))
-    rows = P("dp", SP, None)
+    finer = Mesh(mesh.devices.reshape(4, 4, 2, 2, 2), SP_DP)
+    rows = P(DP, SP, None)
     own = P(SP_DP, None, None)
     placed = (rows,) * 5 + (P(), P(), rows, rows, own, own, own, P())
     return jax.shard_map(shards, mesh=finer, in_specs=placed, out_specs=rows, check_vma=False)

time: 152 us -> 152 us (level)
  no operation moved by 1% of the time
where the time goes in v7:
time: 152 us
  blocking collectives  136 us (89%)
  Pallas kernels  15.4 us (10%)
    all_to_all x4, blocking collectives, exchange(): return lax.all_to_all(x, axes, split_axis=0, concat_axis=0, tiled=True)  136 us
    pallas_call x1, Pallas kernels, expert(): call(expert_body, jax.ShapeDtypeStruct(fours.shape, fours.dtype), 30, gri...  5.51 us
    pallas_call x1, Pallas kernels, attend(): call(attend_body, (jax.ShapeDtypeStruct((parts, rows, size), qkv.dtype),...  3.45 us

profile of v7, /device:TPU:1, one launch (start us, length us, event | category | flops | bytes accessed | tf_op | source)
XLA Modules:
  0.0 151.8 jit_solution(15960613594525537100)
XLA Ops:
  0.0 0.0 copy-start.6
  0.0 1.5 shard_map.127
  1.5 30.0 %all_to_all.20.qkv_ref = bf16[16,3,128,128]{3,2,1,0:T(8,128)(2,1)S(1)} all-to-all(bf16[16,3,128,128]{3,2,1,0:T(8,128)(2,1)S(1)} %shard_map.127), channel_id=1, replica_groups=mesh['sp_0'=4,'sp_1'=4,'x_1'=2,'x_0'=2,'core'=2] {'sp_0','sp_1'}, dimensions={0} | all-to-all | bytes 3145728 | tf_op jit(solution)/shard_map/all_to_all | solution.py:342
  31.5 0.0 copy-done.6
  31.5 0.0 copy-start.3
  31.5 0.0 copy-start.4
  31.6 0.0 copy-start.7
  31.6 0.0 copy-start.8
  31.6 3.4 %shard_map.128 = (bf16[16,128,128]{2,1,0:T(8,128)(2,1)S(1)}, bf16[2048,2048]{1,0:T(8,128)(2,1)S(1)}) custom-call(bf16[16,3,128,128]{3,2,1,0:T(8,128)(2,1)S(1)} %all_to_all.20.qkv_ref, f32[1,2048]{1,0:T(1,128)S(1)} %bitcast.11, bf16[2048,2048]{1,0:T(8,128)(2,1)} %weight_ref.1), custom_call_target="tpu_custom_call" | custom-call | tf_op jit(solution)/shard_map/pallas_call | solution.py:134
  35.0 13.3 %all_to_all.21.heads_ref = bf16[16,128,128]{2,1,0:T(8,128)(2,1)S(1)} all-to-all(bf16[16,128,128]{2,1,0:T(8,128)(2,1)S(1)} %get-tuple-element.10), channel_id=1, replica_groups=mesh['sp_0'=4,'sp_1'=4,'x_1'=2,'x_0'=2,'core'=2] {'sp_0','sp_1'}, dimensions={0} | all-to-all | bytes 1048576 | tf_op jit(solution)/shard_map/all_to_all | solution.py:342
  48.3 0.0 copy-done.3
  48.4 0.0 copy-done.4
  48.4 0.0 copy-done.7
  48.4 0.0 copy-done.8
  48.4 2.8 %shard_map.129 = (bf16[128,2048]{1,0:T(8,128)(2,1)S(1)}, bf16[128,12,8,128]{3,2,1,0:T(8,128)(2,1)S(1)}, bf16[4,128,1024]{2,1,0:T(8,128)(2,1)S(1)}) custom-call(bf16[16,128,128]{2,1,0:T(8,128)(2,1)S(1)} %all_to_all.21.heads_ref, bf16[1,128,2048]{2,1,0:T(8,128)(2,1)S(1)} %copy-done.3, bf16[2048,2048]{1,0:T(8,128)(2,1)S(1)} %get-tuple-element.11.weight_ref, ...), custom_call_target="tpu_custom_call" | custom-call | tf_op jit(solution)/shard_map/pallas_call | solution.py:233
  51.2 0.0 copy-start
  51.2 0.0 copy-start.1
  51.2 0.0 copy-start.2
  51.2 47.3 %all_to_all.22 = bf16[128,12,8,128]{3,2,1,0:T(8,128)(2,1)S(1)} all-to-all(bf16[128,12,8,128]{3,2,1,0:T(8,128)(2,1)S(1)} %get-tuple-element.12), channel_id=1, replica_groups=mesh['sp_0'=4,'sp_1'=4,'x_1'=2,'x_0'=2,'core'=2] {'x_0','x_1','core','sp..., dimensions={0} | all-to-all | bytes 6291456 | tf_op jit(solution)/shard_map/all_to_all | solution.py:342
  98.5 0.0 copy-done
  98.5 0.0 copy-done.1
  98.5 0.0 copy-done.2
  98.5 5.5 %shard_map.130 = bf16[32,4,12,8,128]{4,3,2,1,0:T(8,128)(2,1)S(1)} custom-call(bf16[32,4,12,8,128]{4,3,2,1,0:T(8,128)(2,1)S(1)} %bitcast.7, bf16[1,2048,512]{2,1,0:T(8,128)(2,1)S(1)} %copy-done, bf16[1,2048,512]{2,1,0:T(8,128)(2,1)S(1)} %copy-done.1, bf16[1,512,2048]{2,1,0:T(8,128)(2,1)S(1)} %copy-done.2), custom_call_target="tpu_custom_call" | custom-call | tf_op jit(solution)/shard_map/pallas_call | solution.py:306
  104.0 0.0 copy-start.5
  104.0 45.6 %all_to_all.23.in_ref = bf16[128,12,8,128]{3,2,1,0:T(8,128)(2,1)S(1)} all-to-all(bf16[128,12,8,128]{3,2,1,0:T(8,128)(2,1)S(1)} %bitcast.8), channel_id=1, replica_groups=mesh['sp_0'=4,'sp_1'=4,'x_1'=2,'x_0'=2,'core'=2] {'x_0','x_1','core','sp..., dimensions={0} | all-to-all | bytes 6291456 | tf_op jit(solution)/shard_map/all_to_all | solution.py:342
  149.7 0.0 copy-done.5
  149.7 2.1 %shard_map.131 = bf16[1,128,2048]{2,1,0:T(8,128)(2,1)} custom-call(bf16[128,12,8,128]{3,2,1,0:T(8,128)(2,1)S(1)} %all_to_all.23.in_ref, bf16[4,128,1024]{2,1,0:T(8,128)(2,1)S(1)} %get-tuple-element.13.blend_ref, bf16[128,2048]{1,0:T(8,128)(2,1)S(1)} %get-tuple-element.14.first_ref, f32[1,2048]{1,0:T(1,128)S(1)} %bitcast.10), custom_call_target="tpu_custom_call" | custom-call | tf_op jit(solution)/shard_map/pallas_call | solution.py:334
Async XLA Ops:
  0.0 31.5 %copy-start.6 = (f32[1,1,2048]{2,1,0:T(1,128)S(1)}, f32[1,1,2048]{2,1,0:T(1,128)}, u32[]{:S(2)}) copy-start(f32[1,1,2048]{2,1,0:T(1,128)} %param.17) | copy-start | bytes 24580
  31.5 16.8 %copy-start.3 = (bf16[1,128,2048]{2,1,0:T(8,128)(2,1)S(1)}, bf16[1,128,2048]{2,1,0:T(8,128)(2,1)}, u32[]{:S(2)}) copy-start(bf16[1,128,2048]{2,1,0:T(8,128)(2,1)} %stream_ref.1) | copy-start | bytes 1572868
  31.5 16.8 %copy-start.4 = (f32[2048]{0:T(1024)S(1)}, f32[2048]{0:T(1024)}, u32[]{:S(2)}) copy-start(f32[2048]{0:T(1024)} %param.19) | copy-start | bytes 24580
  31.6 16.8 %copy-start.7 = (s32[1,128,4]{1,2,0:T(4,128)S(1)}, s32[1,128,4]{1,2,0:T(4,128)}, u32[]{:S(2)}) copy-start(s32[1,128,4]{1,2,0:T(4,128)} %param.20) | copy-start | bytes 6148
  31.6 16.8 %copy-start.8 = (f32[1,128,4]{1,2,0:T(4,128)S(1)}, f32[1,128,4]{1,2,0:T(4,128)}, u32[]{:S(2)}) copy-start(f32[1,128,4]{1,2,0:T(4,128)} %param.21) | copy-start | bytes 6148
  51.2 47.3 %copy-start = (bf16[1,2048,512]{2,1,0:T(8,128)(2,1)S(1)}, bf16[1,2048,512]{2,1,0:T(8,128)(2,1)}, u32[]{:S(2)}) copy-start(bf16[1,2048,512]{2,1,0:T(8,128)(2,1)} %gate_ref.1) | copy-start | bytes 6291460
  51.2 47.3 %copy-start.1 = (bf16[1,2048,512]{2,1,0:T(8,128)(2,1)S(1)}, bf16[1,2048,512]{2,1,0:T(8,128)(2,1)}, u32[]{:S(2)}) copy-start(bf16[1,2048,512]{2,1,0:T(8,128)(2,1)} %up_ref.1) | copy-start | bytes 6291460
  51.2 47.3 %copy-start.2 = (bf16[1,512,2048]{2,1,0:T(8,128)(2,1)S(1)}, bf16[1,512,2048]{2,1,0:T(8,128)(2,1)}, u32[]{:S(2)}) copy-start(bf16[1,512,2048]{2,1,0:T(8,128)(2,1)} %down_ref.1) | copy-start | bytes 6291460
  104.0 45.6 %copy-start.5 = (f32[2048]{0:T(1024)S(1)}, f32[2048]{0:T(1024)}, u32[]{:S(2)}) copy-start(f32[2048]{0:T(1024)} %param.25) | copy-start | bytes 24580

commit v8 on v6

--- a/solution.py
+++ b/solution.py
@@ -106,16 +106,15 @@
                 top = jnp.maximum(top, s[:, c * LANE : (c + 1) * LANE])
         return jnp.max(top, axis=1, keepdims=True)
 
+    ones = jnp.ones((block, LANE), jnp.bfloat16)
+
     def blend_rows(b, row_max):
-        total = jnp.zeros((block, LANE), jnp.float32)
-        blended = jnp.zeros((block, size), jnp.float32)
+        blended = jnp.zeros((block, size + LANE), jnp.float32)
         for j in range(b + 1):
             w = jnp.exp2(score_ref[b % 2, :, block * j : block * (j + 1)] - row_max)
-            for c in range(block // LANE):
-                total = total + w[:, c * LANE : (c + 1) * LANE]
-            blended = blended + dot(w.astype(jnp.bfloat16), part(j, 2))
-        row_total = jnp.sum(total, axis=1, keepdims=True)
-        done = (blended / row_total).astype(jnp.bfloat16)
+            sides = jnp.concatenate([part(j, 2), ones], axis=1)
+            blended = blended + dot(w.astype(jnp.bfloat16), sides)
+        done = (blended[:, :size] / blended[:, size:]).astype(jnp.bfloat16)
         out_ref[pair * b : pair * (b + 1)] = done.reshape(pair, rows, size)
 
     last = parts // pair - 1

time: 152 us -> 152 us (level)
  no operation moved by 1% of the time
where the time goes in v8:
time: 152 us
  blocking collectives  136 us (89%)
  Pallas kernels  15.4 us (10%)
    all_to_all x4, blocking collectives, exchange(): return lax.all_to_all(x, axes, split_axis=0, concat_axis=0, tiled=True)  136 us
    pallas_call x1, Pallas kernels, expert(): call(expert_body, jax.ShapeDtypeStruct(fours.shape, fours.dtype), 30, gri...  5.51 us
    pallas_call x1, Pallas kernels, attend(): call(attend_body, (jax.ShapeDtypeStruct((parts, rows, size), qkv.dtype),...  3.45 us

profile of v8, /device:TPU:1, one launch (start us, length us, event | category | flops | bytes accessed | tf_op | source)
XLA Modules:
  0.0 151.8 jit_solution(12545646767883254712)
XLA Ops:
  0.0 0.0 copy-start.6
  0.0 1.5 shard_map.127
  1.5 30.0 %all_to_all.20.qkv_ref = bf16[16,3,128,128]{3,2,1,0:T(8,128)(2,1)S(1)} all-to-all(bf16[16,3,128,128]{3,2,1,0:T(8,128)(2,1)S(1)} %shard_map.127), channel_id=1, replica_groups=mesh['sp_0'=4,'sp_1'=4,'dp'=8] {'sp_0','sp_1'}, dimensions={0} | all-to-all | bytes 3145728 | tf_op jit(solution)/shard_map/all_to_all | solution.py:336
  31.5 0.0 copy-done.6
  31.5 0.0 copy-start.3
  31.5 0.0 copy-start.4
  31.6 0.0 copy-start.7
  31.6 0.0 copy-start.8
  31.6 3.4 %shard_map.128 = (bf16[16,128,128]{2,1,0:T(8,128)(2,1)S(1)}, bf16[2048,2048]{1,0:T(8,128)(2,1)S(1)}) custom-call(bf16[16,3,128,128]{3,2,1,0:T(8,128)(2,1)S(1)} %all_to_all.20.qkv_ref, f32[1,2048]{1,0:T(1,128)S(1)} %bitcast.11, bf16[2048,2048]{1,0:T(8,128)(2,1)} %weight_ref.1), custom_call_target="tpu_custom_call" | custom-call | tf_op jit(solution)/shard_map/pallas_call | solution.py:132
  35.0 13.3 %all_to_all.21.heads_ref = bf16[16,128,128]{2,1,0:T(8,128)(2,1)S(1)} all-to-all(bf16[16,128,128]{2,1,0:T(8,128)(2,1)S(1)} %get-tuple-element.10), channel_id=1, replica_groups=mesh['sp_0'=4,'sp_1'=4,'dp'=8] {'sp_0','sp_1'}, dimensions={0} | all-to-all | bytes 1048576 | tf_op jit(solution)/shard_map/all_to_all | solution.py:336
  48.3 0.0 copy-done.3
  48.4 0.0 copy-done.4
  48.4 0.0 copy-done.7
  48.4 0.0 copy-done.8
  48.4 2.8 %shard_map.129 = (bf16[128,2048]{1,0:T(8,128)(2,1)S(1)}, bf16[128,12,8,128]{3,2,1,0:T(8,128)(2,1)S(1)}, bf16[4,128,1024]{2,1,0:T(8,128)(2,1)S(1)}) custom-call(bf16[16,128,128]{2,1,0:T(8,128)(2,1)S(1)} %all_to_all.21.heads_ref, bf16[1,128,2048]{2,1,0:T(8,128)(2,1)S(1)} %copy-done.3, bf16[2048,2048]{1,0:T(8,128)(2,1)S(1)} %get-tuple-element.11.weight_ref, ...), custom_call_target="tpu_custom_call" | custom-call | tf_op jit(solution)/shard_map/pallas_call | solution.py:228
  51.2 0.0 copy-start
  51.2 0.0 copy-start.1
  51.2 0.0 copy-start.2
  51.2 47.6 %all_to_all.22 = bf16[128,12,8,128]{3,2,1,0:T(8,128)(2,1)S(1)} all-to-all(bf16[128,12,8,128]{3,2,1,0:T(8,128)(2,1)S(1)} %get-tuple-element.12), channel_id=1, replica_groups=mesh['sp_0'=4,'sp_1'=4,'dp'=8] {'dp','sp_0','sp_1'}, dimensions={0} | all-to-all | bytes 6291456 | tf_op jit(solution)/shard_map/all_to_all | solution.py:336
  98.8 0.0 copy-done
  98.8 0.0 copy-done.1
  98.8 0.0 copy-done.2
  98.8 5.5 %shard_map.130 = bf16[32,4,12,8,128]{4,3,2,1,0:T(8,128)(2,1)S(1)} custom-call(bf16[32,4,12,8,128]{4,3,2,1,0:T(8,128)(2,1)S(1)} %bitcast.7, bf16[1,2048,512]{2,1,0:T(8,128)(2,1)S(1)} %copy-done, bf16[1,2048,512]{2,1,0:T(8,128)(2,1)S(1)} %copy-done.1, bf16[1,512,2048]{2,1,0:T(8,128)(2,1)S(1)} %copy-done.2), custom_call_target="tpu_custom_call" | custom-call | tf_op jit(solution)/shard_map/pallas_call | solution.py:300
  104.3 0.0 copy-start.5
  104.3 45.4 %all_to_all.23.in_ref = bf16[128,12,8,128]{3,2,1,0:T(8,128)(2,1)S(1)} all-to-all(bf16[128,12,8,128]{3,2,1,0:T(8,128)(2,1)S(1)} %bitcast.8), channel_id=1, replica_groups=mesh['sp_0'=4,'sp_1'=4,'dp'=8] {'dp','sp_0','sp_1'}, dimensions={0} | all-to-all | bytes 6291456 | tf_op jit(solution)/shard_map/all_to_all | solution.py:336
  149.7 0.0 copy-done.5
  149.7 2.1 %shard_map.131 = bf16[1,128,2048]{2,1,0:T(8,128)(2,1)} custom-call(bf16[128,12,8,128]{3,2,1,0:T(8,128)(2,1)S(1)} %all_to_all.23.in_ref, bf16[4,128,1024]{2,1,0:T(8,128)(2,1)S(1)} %get-tuple-element.13.blend_ref, bf16[128,2048]{1,0:T(8,128)(2,1)S(1)} %get-tuple-element.14.first_ref, f32[1,2048]{1,0:T(1,128)S(1)} %bitcast.10), custom_call_target="tpu_custom_call" | custom-call | tf_op jit(solution)/shard_map/pallas_call | solution.py:328
Async XLA Ops:
  0.0 31.5 %copy-start.6 = (f32[1,1,2048]{2,1,0:T(1,128)S(1)}, f32[1,1,2048]{2,1,0:T(1,128)}, u32[]{:S(2)}) copy-start(f32[1,1,2048]{2,1,0:T(1,128)} %param.17) | copy-start | bytes 24580
  31.5 16.8 %copy-start.3 = (bf16[1,128,2048]{2,1,0:T(8,128)(2,1)S(1)}, bf16[1,128,2048]{2,1,0:T(8,128)(2,1)}, u32[]{:S(2)}) copy-start(bf16[1,128,2048]{2,1,0:T(8,128)(2,1)} %stream_ref.1) | copy-start | bytes 1572868
  31.5 16.8 %copy-start.4 = (f32[2048]{0:T(1024)S(1)}, f32[2048]{0:T(1024)}, u32[]{:S(2)}) copy-start(f32[2048]{0:T(1024)} %param.19) | copy-start | bytes 24580
  31.6 16.8 %copy-start.7 = (s32[1,128,4]{1,2,0:T(4,128)S(1)}, s32[1,128,4]{1,2,0:T(4,128)}, u32[]{:S(2)}) copy-start(s32[1,128,4]{1,2,0:T(4,128)} %param.20) | copy-start | bytes 6148
  31.6 16.8 %copy-start.8 = (f32[1,128,4]{1,2,0:T(4,128)S(1)}, f32[1,128,4]{1,2,0:T(4,128)}, u32[]{:S(2)}) copy-start(f32[1,128,4]{1,2,0:T(4,128)} %param.21) | copy-start | bytes 6148
  51.2 47.6 %copy-start = (bf16[1,2048,512]{2,1,0:T(8,128)(2,1)S(1)}, bf16[1,2048,512]{2,1,0:T(8,128)(2,1)}, u32[]{:S(2)}) copy-start(bf16[1,2048,512]{2,1,0:T(8,128)(2,1)} %gate_ref.1) | copy-start | bytes 6291460
  51.2 47.6 %copy-start.1 = (bf16[1,2048,512]{2,1,0:T(8,128)(2,1)S(1)}, bf16[1,2048,512]{2,1,0:T(8,128)(2,1)}, u32[]{:S(2)}) copy-start(bf16[1,2048,512]{2,1,0:T(8,128)(2,1)} %up_ref.1) | copy-start | bytes 6291460
  51.2 47.6 %copy-start.2 = (bf16[1,512,2048]{2,1,0:T(8,128)(2,1)S(1)}, bf16[1,512,2048]{2,1,0:T(8,128)(2,1)}, u32[]{:S(2)}) copy-start(bf16[1,512,2048]{2,1,0:T(8,128)(2,1)} %down_ref.1) | copy-start | bytes 6291460
  104.3 45.4 %copy-start.5 = (f32[2048]{0:T(1024)S(1)}, f32[2048]{0:T(1024)}, u32[]{:S(2)}) copy-start(f32[2048]{0:T(1024)} %param.25) | copy-start | bytes 24580
